TPU v7x, 512 devices: a whole 4x8x8 slice. The times are simulated.
512 devices in a mesh: ep: 32 (over z, x), tp: 16 (over y, core).
Axes of the slice: x: 4, y: 8, z: 8, core: 2. Of those that a mesh axis runs over, the one named last changes fastest.
Arguments:
- x_in: bfloat16 [4096, 12288], P('tp', 'ep'), may hold values from -6 to 6
- z_in: bfloat16 [4096, 12288], P('tp', 'ep'), may hold values from -6 to 6
- dt_raw: float32 [64, 12288], P('tp', 'ep'), may hold values from -6 to 6
- decay_rate: float32 [64], P('tp'), may hold values from 0 to 1, as said below
- b_in: bfloat16 [256, 12288], P(None, 'ep'), may hold values from -6 to 6
- c_in: bfloat16 [256, 12288], P(None, 'ep'), may hold values from -6 to 6
- conv_x: float32 [4096, 4], P('tp'), may hold values from -3 to 3
- conv_b: float32 [256, 4], replicated, may hold values from -3 to 3
- conv_c: float32 [256, 4], replicated, may hold values from -3 to 3
- head_gain: float32 [4096], P('tp'), may hold values from 0.1 to 1.9
- moe_rows: bfloat16 [5120, 2048], P('ep'), may hold values from -6 to 6
- moe_gain: float32 [2048], replicated, may hold values from 0.1 to 1.9
- routes: int32 [5120, 2], P('ep'), may hold values from 0 to 31, all different within a row; in each aligned block of 160 rows (0 to 159, 160 to 319, ...) at most 20 rows name the same one
- route_logit: float32 [5120, 2], P('ep'), may hold values from -6 to 6
- w_gate: bfloat16 [32, 2048, 5120], P('ep', None, 'tp'), may hold values from -0.125 to 0.125
- w_up: bfloat16 [32, 2048, 5120], P('ep', None, 'tp'), may hold values from -0.125 to 0.125
- w_down: bfloat16 [32, 5120, 2048], P('ep', 'tp'), may hold values from -0.078125 to 0.078125
Outputs:
- mixed: bfloat16 [4096, 12288], P('tp', 'ep')
- moe_out: bfloat16 [2048, 5120], P('tp', 'ep')
Inputs may be any that keep to these rules, and one draw needn't show every extreme that they name: `routes`: each row names 2 different experts; among the rows of one index of ep no expert is named more than 20 times, a bound that some block reaches. `decay_rate`: positive rates.
All inputs are finite; a program needn't handle non-finite values.
Results may differ from a plain program's by a relative error of at most 0.018.
Values may be sent and summed in bfloat16 or wider, within the bound.
No kernel may reach another device: no remote copies, remote signals or barrier semaphores. Data moves between devices by JAX's collectives and lax.ppermute only.
A program may use at most 64 MiB of HBM per device.

v0:
```python
import jax
import jax.numpy as jnp
from jax import lax
from jax.sharding import Mesh
from jax.sharding import PartitionSpec as P

HEADS = 64
HEAD_DIM = 64
GROUPS = 2
NSTATE = 128
BLOCK = 128
EXP_DEV = 1
EP = ("ep_0", "ep_1")


HIGHEST = lax.Precision.HIGHEST
ROW_EPS = 0.1
HEAD_EPS = 1.0


def from_behind(value, axis, steps):
    count = lax.axis_size(axis)
    initial, last = (max(0, -steps), min(count, count - steps))
    return lax.ppermute(value, axis, [(source, source + steps) for source in range(initial, last)])


def filled_with(shard, identity):
    return jax.tree.map(
        lambda a, e: jnp.broadcast_to(jnp.asarray(e, a.dtype), a.shape), shard, identity
    )


def entering(shard, axes, combine, identity):
    before = start = filled_with(shard, identity)
    total = shard
    for axis in reversed(axes):
        size, mine = (lax.axis_size(axis), lax.axis_index(axis))
        pieces = jax.tree.map(
            lambda part, kind: lax.all_gather(part.astype(kind), axis),
            total,
            (jnp.bfloat16, jnp.bfloat16),
        )
        inside, total = (start, start)
        for k in range(size):
            passed = k < mine
            total = combine(
                total, jax.tree.map(lambda part, own: part[k].astype(own.dtype), pieces, shard)
            )
            inside = jax.tree.map(lambda new, old: jnp.where(passed, new, old), total, inside)
        before = combine(inside, before)
    return before


def in_blocks(shard, dim, size):
    before, after = (shard.shape[:dim], shard.shape[dim + 1 :])
    return jnp.moveaxis(shard.reshape(*before, size, -1, *after), dim, 0)


def sent_and_summed(shard, axis, dim):
    tiles = in_blocks(shard, dim, lax.axis_size(axis))
    arrived = lax.all_to_all(tiles, axis, split_axis=0, concat_axis=0, tiled=True)
    return arrived.astype(jnp.float32).sum(axis=0)


def conv_with_rims(signal, rim_rows, weight):
    taps = weight.shape[1]
    length = signal.shape[1]
    joined = jnp.concatenate([rim_rows.astype(jnp.float32), signal.astype(jnp.float32)], axis=1)
    running = jnp.zeros(signal.shape, jnp.float32)
    for offset in range(taps):
        running = running + weight[:, offset : offset + 1] * joined[:, offset : offset + length]
    return jax.nn.silu(running)


def block_step(state_in, x_block, b_block, c_block, log_block, step_block):
    cum_log = jnp.cumsum(log_block, axis=1)
    seg_log = cum_log[:, :, None] - cum_log[:, None, :]
    causal = jnp.tril(jnp.ones((log_block.shape[1], log_block.shape[1]), bool))
    decay_mask = jnp.exp(jnp.where(causal[None], seg_log, -jnp.inf))
    scores = (
        jnp.einsum("hnt,hns->hts", c_block, b_block, precision=HIGHEST)
        * decay_mask
        * step_block[:, None, :]
    )
    inner_term = jnp.einsum("hts,hps->hpt", scores, x_block, precision=HIGHEST)
    carried = (
        jnp.einsum("hnt,hpn->hpt", c_block, state_in, precision=HIGHEST)
        * jnp.exp(cum_log)[:, None, :]
    )
    tail_weight = jnp.exp(cum_log[:, -1:] - cum_log) * step_block
    fresh_state = jnp.einsum(
        "hps,hns->hpn", x_block * tail_weight[:, None, :], b_block, precision=HIGHEST
    )
    new_state = jnp.exp(cum_log[:, -1])[:, None, None] * state_in + fresh_state
    return (new_state, inner_term + carried)


def combine_states(before_part, after_part):
    return (
        before_part[0] * after_part[0],
        after_part[0][..., None, None] * before_part[1] + after_part[1],
    )


def mixer_half(x_in, z_in, dt_raw, decay_rate, b_in, c_in, conv_x, conv_b, conv_c, head_gain):
    head_count = dt_raw.shape[0]
    length = dt_raw.shape[1]
    taps = conv_x.shape[1]
    value_rows = x_in.shape[0]
    per_group = HEADS // GROUPS
    group_index = lax.axis_index("tp") * head_count // per_group
    b_own = lax.dynamic_slice_in_dim(b_in, group_index * NSTATE, NSTATE, 0)
    c_own = lax.dynamic_slice_in_dim(c_in, group_index * NSTATE, NSTATE, 0)
    taps_b = lax.dynamic_slice_in_dim(conv_b, group_index * NSTATE, NSTATE, 0)
    taps_c = lax.dynamic_slice_in_dim(conv_c, group_index * NSTATE, NSTATE, 0)
    edge = length - taps + 1
    own_rims = jnp.concatenate([x_in[:, edge:], b_own[:, edge:], c_own[:, edge:]], axis=0)
    rims = from_behind(own_rims, EP, 1)
    x_conv = conv_with_rims(x_in, rims[:value_rows], conv_x).reshape(head_count, HEAD_DIM, length)
    b_conv = conv_with_rims(b_own, rims[value_rows : value_rows + NSTATE], taps_b)
    c_conv = conv_with_rims(c_own, rims[value_rows + NSTATE :], taps_c)
    step_dt = jax.nn.softplus(dt_raw)
    log_decay = -step_dt * decay_rate[:, None]
    block_count = length // BLOCK

    def blocks(tensor):
        return jnp.moveaxis(tensor.reshape(tensor.shape[:-1] + (block_count, BLOCK)), -2, 0)

    def spread_heads(tensor):
        return jnp.broadcast_to(tensor[None], (head_count,) + tensor.shape)

    def advance(state_in, inputs):
        x_block, b_block, c_block, log_block, step_block = inputs
        return block_step(
            state_in, x_block, spread_heads(b_block), spread_heads(c_block), log_block, step_block
        )

    init_state = jnp.zeros((head_count, HEAD_DIM, NSTATE), jnp.float32)
    local_state, block_out = lax.scan(
        advance,
        init_state,
        (blocks(x_conv), blocks(b_conv), blocks(c_conv), blocks(log_decay), blocks(step_dt)),
    )
    y_local = jnp.moveaxis(block_out, 0, -2).reshape(head_count, HEAD_DIM, length)
    total_decay = jnp.exp(jnp.sum(log_decay, axis=1))
    _, incoming = entering(
        (total_decay, local_state),
        EP,
        combine_states,
        (jnp.ones_like(total_decay), jnp.zeros_like(local_state)),
    )
    reach_decay = jnp.exp(jnp.cumsum(log_decay, axis=1))
    carried = (
        jnp.einsum("nt,hpn->hpt", c_conv, incoming, precision=HIGHEST) * reach_decay[:, None, :]
    )
    y_mixed = y_local + carried
    gated_out = y_mixed * jax.nn.silu(
        z_in.astype(jnp.float32).reshape(head_count, HEAD_DIM, length)
    )
    head_scale = lax.rsqrt(jnp.mean(gated_out * gated_out, axis=1, keepdims=True) + HEAD_EPS)
    normed_out = gated_out * head_scale * head_gain.reshape(head_count, HEAD_DIM, 1)
    return normed_out.reshape(head_count * HEAD_DIM, length).astype(jnp.bfloat16)


def experts_half(moe_rows, moe_gain, routes, route_logit, w_gate, w_up, w_down):
    tokens = moe_rows.shape[0]
    top_count = routes.shape[1]
    features = moe_gain.shape[0]
    experts = EXP_DEV * lax.axis_size(EP)
    capacity = 2 * tokens * top_count // experts
    col_width = features // lax.axis_size("tp")
    rows_float = moe_rows.astype(jnp.float32)
    row_scale = lax.rsqrt(jnp.mean(rows_float * rows_float, axis=1, keepdims=True) + ROW_EPS)
    normed_float = rows_float * row_scale * moe_gain
    flat_routes = routes.reshape(-1)
    hit_table = (flat_routes[:, None] == jnp.arange(experts, dtype=jnp.int32)[None, :]).astype(
        jnp.int32
    )
    slot_rank = jnp.sum((jnp.cumsum(hit_table, axis=0) - hit_table) * hit_table, axis=1)
    slot_index = flat_routes * capacity + slot_rank
    owner_row = jnp.arange(tokens * top_count, dtype=jnp.int32) // top_count
    column = lax.axis_index("tp") * col_width
    normed = lax.dynamic_slice_in_dim(normed_float.astype(jnp.bfloat16), column, col_width, 1)
    outbox = (
        jnp.zeros((experts * capacity, col_width), jnp.bfloat16)
        .at[slot_index]
        .set(normed[owner_row])
    )
    arrived = lax.all_to_all(
        outbox.reshape(experts, capacity, col_width), EP, split_axis=0, concat_axis=0, tiled=True
    ).reshape(-1, col_width)
    part_rows = lax.all_gather(arrived, "tp", axis=1, tiled=True)
    gate_rows = w_gate[0]
    up_rows = w_up[0]
    gate_act = jnp.dot(part_rows, gate_rows, preferred_element_type=jnp.float32)
    up_act = jnp.dot(part_rows, up_rows, preferred_element_type=jnp.float32)
    hidden = (jax.nn.silu(gate_act) * up_act).astype(jnp.bfloat16)
    columns = w_down[0]
    summed = sent_and_summed(
        lax.dot_general(
            columns, hidden, (((0,), (1,)), ((), ())), preferred_element_type=jnp.float32
        ).astype(jnp.bfloat16),
        "tp",
        0,
    )
    expert_out = summed.astype(jnp.bfloat16).reshape(col_width, experts, capacity)
    returned = lax.all_to_all(expert_out, EP, split_axis=1, concat_axis=1, tiled=True)
    picked = returned.reshape(col_width, experts * capacity)[:, slot_index].astype(jnp.float32)
    picked = picked.reshape(col_width, tokens, top_count)
    weight = jax.nn.sigmoid(route_logit - route_logit[:, ::-1])
    combined = jnp.sum(picked * weight[None], axis=2)
    return combined.astype(jnp.bfloat16)


def on_device(
    x_in,
    z_in,
    dt_raw,
    decay_rate,
    b_in,
    c_in,
    conv_x,
    conv_b,
    conv_c,
    head_gain,
    moe_rows,
    moe_gain,
    routes,
    route_logit,
    w_gate,
    w_up,
    w_down,
):
    mixed = mixer_half(
        x_in, z_in, dt_raw, decay_rate, b_in, c_in, conv_x, conv_b, conv_c, head_gain
    )
    moe_out = experts_half(moe_rows, moe_gain, routes, route_logit, w_gate, w_up, w_down)
    return (mixed, moe_out)


def solution(mesh):
    finer = Mesh(mesh.devices.reshape(8, 4, mesh.shape["tp"]), ("ep_0", "ep_1", "tp"))
    in_specs = (
        P("tp", EP),
        P("tp", EP),
        P("tp", EP),
        P("tp"),
        P(None, EP),
        P(None, EP),
        P("tp", None),
        P(),
        P(),
        P("tp"),
        P(EP, None),
        P(),
        P(EP, None),
        P(EP, None),
        P(EP, None, "tp"),
        P(EP, None, "tp"),
        P(EP, "tp", None),
    )
    out_specs = (P("tp", EP), P("tp", EP))
    return jax.shard_map(
        on_device, mesh=finer, in_specs=in_specs, out_specs=out_specs, check_vma=False
    )
```

profile of v0, /device:TPU:24, one launch (start us, length us, event | category | flops | bytes accessed | tf_op | source)
XLA Modules:
  0.0 194.1 jit_solution(6418290742828513007)
XLA Ops:
  7.2 1.3 convert_element_type.375
  8.6 0.2 multiply_reduce_fusion
  9.0 0.1 eq.22
  9.2 0.9 reduce-window.16
  10.0 0.2 slice_reduce_fusion.1
  10.5 0.1 mul.536
  10.8 0.8 dynamic-slice.1
  11.7 2.1 %scatter_custom_fusion = bf16[640,128]{1,0:T(8,128)(2,1)S(1)} fusion(s32[320]{0:T(512)S(1)} %get-tuple-element.144, bf16[160,128]{1,0:T(8,128)(2,1)S(1)} %fusion.96, s32[1024]{0:T(1024)S(1)} %pad_clamp_fusion.1, bf16[]{:T(256)} %constant.124.clone.1), kind=kCustom, calls=%fused_computation.142 | custom fusion | bytes 163842 | tf_op jit(solution)/shard_map/scatter | solution.py:187
  13.9 24.6 %all_to_all.15 = bf16[32,20,128]{2,1,0:T(8,128)(2,1)S(1)} all-to-all(bf16[32,20,128]{2,1,0:T(8,128)(2,1)S(1)} %reshape.360), channel_id=1, replica_groups=mesh['ep_0'=8,'ep_1'=4,'tp'=16] {'ep_0','ep_1'}, dimensions={0} | all-to-all | bytes 327680 | tf_op jit(solution)/shard_map/all_to_all | solution.py:189
  38.5 0.7 reshape.361
  39.2 0.9 constant_dynamic-slice_fusion.5
  40.2 0.1 copy.61
  40.6 1.3 dynamic-slice
  42.6 0.2 fusion.133
  42.8 0.2 dynamic-update-slice
  43.0 1.9 collective-permute-start
  44.9 11.5 %all-reduce.1 = bf16[16]{0:T(256)(128)(2,1)S(1)} all-reduce(bf16[16]{0:T(256)(128)(2,1)S(1)} %dynamic-update-slice), channel_id=2, replica_groups=mesh['ep_0'=8,'ep_1'=4,'tp'=16] {'ep_1'}, use_global_device_ids=true, to_apply=%add.1 | all-reduce | flops 16 | bytes 64
  56.4 13.9 %all-gather.2 = bf16[8,1,4]{2,1,0:T(2,128)(2,1)S(1)} all-gather(bf16[1,1,4]{2,1,0:T(2,128)(2,1)S(1)} %bitcast.294), channel_id=1, replica_groups=mesh['ep_0'=8,'ep_1'=4,'tp'=16] {'ep_0'}, dimensions={0}, use_global_device_ids=true | all-gather | bytes 72 | tf_op jit(solution)/shard_map/all_gather | solution.py:39
  70.3 1.2 reduce-window.14
  71.6 0.2 slice_reduce_fusion.2
  71.7 0.2 reduce-window.15
  72.6 0.1 copy.41
  72.7 0.6 divide_multiply_fusion
  73.4 0.2 reshape_reshape.3
  73.5 0.1 divide_multiply_fusion.2
  73.7 0.1 divide_multiply_fusion.1
  73.8 5.1 %all-gather.5.cloned.1.call-done = bf16[640,2048]{1,0:T(8,128)(2,1)} async-done(((bf16[640,128]{1,0:T(8,128)(2,1)}), bf16[640,2048]{1,0:T(8,128)(2,1)}) %all-gather.5.cloned.1.call-update) | async-done | bytes 2621456 | tf_op jit(solution)/shard_map/all_gather | solution.py:192
  79.0 4.3 %fusion.19 = f32[640,320]{0,1:T(8,128)} fusion(bf16[640,2048]{1,0:T(8,128)(2,1)} %all-gather.5.cloned.1.call-done, bf16[1,2048,320]{1,2,0:T(8,128)(2,1)} %param.33), kind=kOutput, calls=%fused_computation.35 | convolution fusion | flops 838860800 | bytes 4751360 | tf_op jit(solution)/shard_map/dot_general | solution.py:195
  83.2 7.1 %fusion.15 = bf16[80,16,8,128]{3,2,1,0:T(8,128)(2,1)} fusion(bf16[1,320,2048]{2,1,0:T(8,128)(2,1)S(1)} %copy-done, bf16[640,2048]{1,0:T(8,128)(2,1)} %all-gather.5.cloned.1.call-done, bf16[1,2048,320]{1,2,0:T(8,128)(2,1)} %param.34, f32[640,320]{0,1:T(8,128)} %fusion.19), kind=kOutput, calls=%fused_computation.31 | convolution fusion | flops 1680261120 | bytes 8683520 | tf_op jit(solution)/shard_map/dot_general | solution.py:200
  90.3 3.9 %copy.73 = bf16[80,16,8,128]{3,2,0,1:T(8,128)(2,1)} copy(bf16[80,16,8,128]{3,2,1,0:T(8,128)(2,1)} %fusion.15) | data formatting | bytes 5242880 | tf_op jit(solution)/shard_map/reshape | solution.py:56
  94.3 5.7 %all-to-all-start.1 = ((bf16[16,128,640]{1,2,0:T(8,128)(2,1)}), bf16[16,128,640]{1,2,0:T(8,128)(2,1)}, u32[]{:S(2)}, u32[]{:S(2)}) async-start(bf16[16,128,640]{1,2,0:T(8,128)(2,1)} %bitcast.276), calls=%async_computation.1 | async-start | bytes 5242880 | tf_op jit(solution)/shard_map/all_to_all | solution.py:61
  100.0 9.7 %while.13 = (s32[]{:T(128)}, f32[4,64,128]{2,1,0:T(8,128)S(1)}, f32[3,4,64,128]{3,2,1,0:T(8,128)S(1)}, f32[3,4,128]{2,1,0:T(4,128)S(1)}, f32[3,4,64,128]{3,0,2,1...) while((s32[]{:T(128)}, f32[4,64,128]{2,1,0:T(8,128)S(1)}, ...), condition=%wide.region_2.3_spmd.clone, body=%wide.region_0.2_spmd.clone.sunk | while | flops 252232192 | bytes 2681072 | solution.py:139
  100.1 0.3 reduce_window_sum.51
  100.4 0.2 slice_reduce_fusion.4
  100.9 0.6 fusion.178
  101.5 0.1 constant_dynamic-slice_fusion.10
  101.6 0.6 fusion.179
  102.3 0.3 fusion.180
  102.6 0.6 convolution_add_fusion.2
  103.3 0.3 reduce_window_sum.51
  103.6 0.2 slice_reduce_fusion.4
  104.1 0.6 fusion.178
  104.7 0.1 constant_dynamic-slice_fusion.10
  104.9 0.6 fusion.179
  105.5 0.3 fusion.180
  105.9 0.6 convolution_add_fusion.2
  106.5 0.3 reduce_window_sum.51
  106.8 0.2 slice_reduce_fusion.4
  107.3 0.6 fusion.178
  108.0 0.1 constant_dynamic-slice_fusion.10
  108.1 0.6 fusion.179
  108.7 0.3 fusion.180
  109.1 0.6 convolution_add_fusion.2
  109.8 12.7 %all-gather.1 = bf16[16,64,128]{2,1,0:T(8,128)(2,1)S(1)} all-gather(bf16[4,64,128]{2,1,0:T(8,128)(2,1)S(1)} %convert_element_type.342), channel_id=3, replica_groups=mesh['ep_0'=8,'ep_1'=4,'tp'=16] {'ep_1'}, dimensions={0}, use_global_device_ids=true | all-gather | bytes 327680 | tf_op jit(solution)/shard_map/all_gather | solution.py:39
  122.5 27.5 %all_gather.25 = bf16[8,4,64,128]{3,2,1,0:T(8,128)(2,1)S(1)} all-gather(bf16[1,4,64,128]{3,2,1,0:T(8,128)(2,1)S(1)} %fusion.74), channel_id=1, replica_groups=mesh['ep_0'=8,'ep_1'=4,'tp'=16] {'ep_0'}, dimensions={0}, use_global_device_ids=true | all-gather | bytes 589824 | tf_op jit(solution)/shard_map/all_gather | solution.py:39
  150.0 0.8 multiply_reduce_fusion.1
  150.9 9.2 %all-to-all-done.1 = bf16[16,128,640]{1,2,0:T(8,128)(2,1)} async-done(((bf16[16,128,640]{1,2,0:T(8,128)(2,1)}), bf16[16,128,640]{1,2,0:T(8,128)(2,1)}, u32[]{:S(2)}, u32[]{:S(2)}) %all-to-all-start.1) | async-done | bytes 2621472 | tf_op jit(solution)/shard_map/all_to_all | solution.py:61
  160.0 2.1 %reduce_sum.64 = bf16[128,640]{0,1:T(8,128)(2,1)S(1)} reduce(bf16[16,128,640]{1,2,0:T(8,128)(2,1)} %all-to-all-done.1, bf16[]{:T(256)} %constant.124.clone.1), dimensions={0}, to_apply=%region_12.13 | reduce | flops 1228800 | bytes 2785282 | tf_op jit(solution)/shard_map/reduce_sum | solution.py:62
  162.2 0.7 reshape.363
  162.9 10.1 %all-to-all-start.2 = ((bf16[128,32,20]{0,2,1:T(8,128)(2,1)}), bf16[128,32,20]{0,2,1:T(8,128)(2,1)S(1)}, u32[]{:S(2)}, u32[]{:S(2)}) async-start(bf16[128,32,20]{0,2,1:T(8,128)(2,1)} %reshape.363), calls=%async_computation.2 | async-start | bytes 393216 | tf_op jit(solution)/shard_map/all_to_all | solution.py:207
  173.0 0.8 multiply_convert_fusion
  173.8 11.1 %all-to-all-done.2 = bf16[128,32,20]{0,2,1:T(8,128)(2,1)S(1)} async-done(((bf16[128,32,20]{0,2,1:T(8,128)(2,1)}), bf16[128,32,20]{0,2,1:T(8,128)(2,1)S(1)}, u32[]{:S(2)}, u32[]{:S(2)}) %all-to-all-start.2) | async-done | bytes 163872 | tf_op jit(solution)/shard_map/all_to_all | solution.py:207
  184.9 1.4 gather_fusion
  186.4 0.9 multiply_reduce_fusion.2
  (99 shorter events, 2.7 us)
Async XLA Ops:
  7.2 76.0 %copy-start = (bf16[1,320,2048]{2,1,0:T(8,128)(2,1)S(1)}, bf16[1,320,2048]{2,1,0:T(8,128)(2,1)}, u32[]{:S(2)}) copy-start(bf16[1,320,2048]{2,1,0:T(8,128)(2,1)} %param.35) | copy-start | bytes 3932164
  7.2 1.4 copy-start.1
  7.2 71.8 %all-gather.5.cloned.1.call-start = ((), (), s32[]{:S(2)}) async-start(), calls=%async_computation.3 | async-start | bytes 2785280 | tf_op jit(solution)/shard_map/all_gather | solution.py:192
  7.2 1.6 copy-start.5
  8.8 30.4 %copy-start.3 = (bf16[256,384]{1,0:T(8,128)(2,1)S(1)}, bf16[256,384]{1,0:T(8,128)(2,1)}, u32[]{:S(2)}) copy-start(bf16[256,384]{1,0:T(8,128)(2,1)} %param.24) | copy-start | bytes 589828
  10.4 30.0 %copy-start.2 = (bf16[256,384]{1,0:T(8,128)(2,1)S(1)}, bf16[256,384]{1,0:T(8,128)(2,1)}, u32[]{:S(2)}) copy-start(bf16[256,384]{1,0:T(8,128)(2,1)} %param.19) | copy-start | bytes 589828
  10.7 31.8 %copy-start.6 = (f32[4,384]{1,0:T(4,128)S(1)}, f32[4,384]{1,0:T(4,128)}, u32[]{:S(2)}) copy-start(f32[4,384]{1,0:T(4,128)} %param.21) | copy-start | bytes 18436
  10.7 31.8 %copy-start.11 = (f32[4]{0:T(128)S(1)}, f32[4]{0:T(128)}, u32[]{:S(2)}) copy-start(f32[4]{0:T(128)} %param.22) | copy-start | bytes 52
  11.6 60.3 %copy-start.4 = (f32[160,2]{0,1:T(2,128)S(1)}, f32[160,2]{0,1:T(2,128)}, u32[]{:S(2)}) copy-start(f32[160,2]{0,1:T(2,128)} %param.32) | copy-start | bytes 3844
  11.6 60.3 %copy-start.8 = (f32[256,4]{0,1:T(4,128)S(1)}, f32[256,4]{0,1:T(4,128)}, u32[]{:S(2)}) copy-start(f32[256,4]{0,1:T(4,128)} %param.27) | copy-start | bytes 12292
  11.6 60.3 %copy-start.9 = (f32[256,4]{0,1:T(4,128)S(1)}, f32[256,4]{0,1:T(4,128)}, u32[]{:S(2)}) copy-start(f32[256,4]{0,1:T(4,128)} %param.26) | copy-start | bytes 12292
  11.7 60.5 %copy-start.7 = (f32[256,4]{0,1:T(4,128)S(1)}, f32[256,4]{0,1:T(4,128)}, u32[]{:S(2)}) copy-start(f32[256,4]{0,1:T(4,128)} %param.25) | copy-start | bytes 12292
  39.2 33.2 %copy-start.10 = (f32[256]{0:T(256)S(1)}, f32[256]{0:T(256)}, u32[]{:S(2)}) copy-start(f32[256]{0:T(256)} %param.28) | copy-start | bytes 3076
  43.0 29.6 %collective-permute-start = (bf16[512,3]{0,1:T(4,128)(2,1)S(1)}, bf16[512,3]{0,1:T(4,128)(2,1)S(1)}, u32[]{:S(2)}, u32[]{:S(2)}) collective-permute-start(bf16[512,3]{0,1:T(4,128)(2,1)S(1)} %pad_maximum_fusion.3), channel_id=1, source_target_pairs={{0,16},{16,32},{32,48},{48,64},{64,80},{80,96},{96,112},{112,128},... | collective-permute-start | bytes 9224 | tf_op jit(solution)/shard_map/ppermute | solution.py:24
  94.3 65.8 %all-to-all-start.1 = ((bf16[16,128,640]{1,2,0:T(8,128)(2,1)}), bf16[16,128,640]{1,2,0:T(8,128)(2,1)}, u32[]{:S(2)}, u32[]{:S(2)}) async-start(bf16[16,128,640]{1,2,0:T(8,128)(2,1)} %bitcast.276), calls=%async_computation.1 | async-start | bytes 5242880 | tf_op jit(solution)/shard_map/all_to_all | solution.py:61
  109.7 40.3 %copy-start.12 = (bf16[256,384]{1,0:T(8,128)(2,1)S(1)}, bf16[256,384]{1,0:T(8,128)(2,1)}, u32[]{:S(2)}) copy-start(bf16[256,384]{1,0:T(8,128)(2,1)} %param.20) | copy-start | bytes 589828
  162.9 22.0 %all-to-all-start.2 = ((bf16[128,32,20]{0,2,1:T(8,128)(2,1)}), bf16[128,32,20]{0,2,1:T(8,128)(2,1)S(1)}, u32[]{:S(2)}, u32[]{:S(2)}) async-start(bf16[128,32,20]{0,2,1:T(8,128)(2,1)} %reshape.363), calls=%async_computation.2 | async-start | bytes 393216 | tf_op jit(solution)/shard_map/all_to_all | solution.py:207
Sparse Core Ops, SparseCore 0:
  39.3 39.5 all-gather.4
where the time goes:
time: 195 us; the launch traced here: 194 us
  blocking collectives  90.1 us (46%)
  waiting for transfers between devices  25.4 us (13%)
  matrix products  18.8 us (10%)
  starting transfers between devices  17.8 us (9%)
  local copies, waits for them, and re-layouts  15.8 us (8%)
  between operations  15.3 us (8%)
  other arithmetic  10.7 us (5%)
    all_gather x3, blocking collectives, entering(): lax.all_gather(part.astype(kind), axis)  54.1 us
    all_to_all x1, blocking collectives, experts_half(): lax.all_to_all(outbox.reshape(experts, capacity, col_width), EP, split_ax...  24.6 us
    unnamed x1, blocking collectives  11.5 us
    all_to_all x1, waiting for transfers between devices, experts_half(): lax.all_to_all(expert_out, EP, split_axis=1, concat_axis=1, tiled=True)  11.1 us
    all_to_all x1, starting transfers between devices, experts_half(): lax.all_to_all(expert_out, EP, split_axis=1, concat_axis=1, tiled=True)  10.1 us
    all_to_all x1, waiting for transfers between devices, sent_and_summed(): lax.all_to_all(tiles, axis, split_axis=0, concat_axis=0, tiled=True)  9.16 us
    dot_general x1, matrix products, experts_half(): lax.dot_general(columns, hidden, (((0,), (1,)), ((), ())), preferred_elem...  7.12 us
    all_to_all x1, starting transfers between devices, sent_and_summed(): lax.all_to_all(tiles, axis, split_axis=0, concat_axis=0, tiled=True)  5.75 us
  transfers between devices with their start and end apart: 4, of which 3 were waited for; matrix products, arithmetic and copies ran while one was open for 9% of the time, Pallas kernels for 0%

commit v1 on v0

v1 whole, which is shorter than its diff:
```python
import jax
import jax.numpy as jnp
from jax import lax
from jax.experimental import pallas as pl
from jax.experimental.pallas import tpu as pltpu
from jax.sharding import Mesh
from jax.sharding import PartitionSpec as P


HEADS = 64
HEAD_DIM = 64
GROUPS = 2
NSTATE = 128
EP = ("z", "x")
TP = ("y", "c")
N_EXP = 32
CAP = 20
HEAD_ROWS = 16
TAIL_ROWS = CAP - HEAD_ROWS
LANES = 128
N_BLK = 8
CHUNK = CAP * N_BLK

TAPS = 4
ROW_EPS = 0.1
HEAD_EPS = 1.0
F32 = jnp.float32
BF16 = jnp.bfloat16
MIB = 1024 * 1024


def iota(shape, dim):
    return lax.broadcasted_iota(jnp.int32, shape, dim)


def dot(a, b):
    return jnp.dot(a, b, preferred_element_type=F32)


def call(kernel, out_shape, args, flops, smem=0, hbm=0, vmem=8, scratch=()):
    specs = [pl.BlockSpec(memory_space=pltpu.SMEM)] * smem
    specs += [pl.BlockSpec(memory_space=pltpu.HBM)] * hbm
    specs += [pl.BlockSpec(memory_space=pltpu.VMEM)] * (len(args) - smem - hbm)
    return pl.pallas_call(
        kernel,
        out_shape=out_shape,
        in_specs=specs,
        out_specs=jax.tree.map(lambda _: pl.BlockSpec(memory_space=pltpu.VMEM), out_shape),
        scratch_shapes=scratch,
        compiler_params=pltpu.CompilerParams(vmem_limit_bytes=vmem * MIB),
        cost_estimate=pl.CostEstimate(flops=flops, bytes_accessed=1 << 20, transcendentals=0),
    )(*args)


def sds(shape, dtype):
    return jax.ShapeDtypeStruct(shape, dtype)


def fetch(pairs, sems):
    copies = [
        pltpu.make_async_copy(source, target, sems.at[k]) for k, (source, target) in enumerate(pairs)
    ]
    for copy in copies:
        copy.start()
    for copy in copies:
        copy.wait()


def store_main(ref, value):
    for j in range(N_BLK):
        ref[:, HEAD_ROWS * j : HEAD_ROWS * (j + 1), :] = value[
            :, LANES * j : LANES * (j + 1)
        ].reshape(N_EXP, HEAD_ROWS, LANES)


def store_tail(ref, value):
    for g in range(2):
        low = N_BLK * HEAD_ROWS + HEAD_ROWS * g
        ref[:, low : low + HEAD_ROWS, :] = value[:, LANES * g : LANES * (g + 1)].reshape(
            N_EXP, HEAD_ROWS, LANES
        )


def load_main(ref):
    return jnp.concatenate(
        [
            ref[:, HEAD_ROWS * j : HEAD_ROWS * (j + 1), :].reshape(N_EXP * HEAD_ROWS, LANES)
            for j in range(N_BLK)
        ],
        axis=1,
    )


def load_tail(ref):
    parts = []
    for g in range(2):
        low = N_BLK * HEAD_ROWS + HEAD_ROWS * g
        parts.append(ref[:, low : low + HEAD_ROWS, :].reshape(N_EXP * HEAD_ROWS, LANES))
    return jnp.concatenate(parts, axis=1)


def prep_kernel(
    core_ref, rows_hbm, gain_hbm, routes_hbm, out_ref, rows_ref, gain_ref, routes_ref, sems
):
    fetch(((rows_hbm, rows_ref), (gain_hbm, gain_ref), (routes_hbm, routes_ref)), sems)
    tokens, features = rows_ref.shape
    half = features // 2
    low = pl.multiple_of(core_ref[0] * half, half)
    rows = rows_ref[...].astype(F32)
    scale = lax.rsqrt(jnp.mean(rows * rows, axis=1, keepdims=True) + ROW_EPS)
    own = rows_ref[:, pl.ds(low, half)].astype(F32)
    normed = (own * scale * gain_ref[:, pl.ds(low, half)]).astype(BF16)
    routes = routes_ref[...]
    expert = iota((N_EXP, tokens), 0)
    picks = [(routes[k : k + 1, :] == expert).astype(F32) for k in range(2)]
    before = (iota((tokens, tokens), 0) < iota((tokens, tokens), 1)).astype(BF16)
    ranks = dot((picks[0] + picks[1]).astype(BF16), before)
    row = iota((N_EXP * HEAD_ROWS, tokens), 0)
    main = jnp.zeros((N_EXP * HEAD_ROWS, tokens), F32)
    tails = [jnp.zeros((N_EXP * HEAD_ROWS, tokens), F32) for _ in range(TAIL_ROWS)]
    for k in range(2):
        rank = jnp.sum(ranks * picks[k], axis=0, keepdims=True).astype(jnp.int32)
        start = routes[k : k + 1, :] * HEAD_ROWS
        in_main = jnp.where(rank < HEAD_ROWS, start + rank, -1)
        in_tail = jnp.where(rank >= HEAD_ROWS, start + rank - HEAD_ROWS, -1000)
        main = main + (row == in_main).astype(F32)
        for q in range(4):
            tails[q] = tails[q] + (row == in_tail + TAIL_ROWS * q).astype(F32)
    store_main(out_ref, dot(main.astype(BF16), normed).astype(BF16))
    tail = jnp.zeros((N_EXP * HEAD_ROWS, 2 * LANES), F32)
    for q in range(4):
        pair = jnp.concatenate(
            [
                normed[:, LANES * q : LANES * (q + 1)],
                normed[:, LANES * (q + 4) : LANES * (q + 5)],
            ],
            axis=1,
        )
        tail = tail + dot(tails[q].astype(BF16), pair)
    store_tail(out_ref, tail.astype(BF16))


def tail_pick(q):
    shape = (N_EXP * TAIL_ROWS, N_EXP * HEAD_ROWS)
    r, col = (iota(shape, 0), iota(shape, 1))
    source = (r // TAIL_ROWS) * HEAD_ROWS + TAIL_ROWS * q + r % TAIL_ROWS
    return (source == col).astype(BF16)


def unpacked(ref):
    tails = load_tail(ref)
    picked = [dot(tail_pick(q), tails).astype(BF16) for q in range(4)]
    tail = jnp.concatenate(
        [p[:, LANES * g : LANES * (g + 1)] for g in range(2) for p in picked], axis=1
    )
    return jnp.concatenate([load_main(ref), tail], axis=0)


def first_half_kernel(core_ref, own_ref, gate_ref, up_ref, gate_out, up_out):
    half = gate_ref.shape[1] // 2
    low = pl.multiple_of(core_ref[0] * half, half)
    rows = unpacked(own_ref)
    gate_out[...] = over_last(rows, gate_ref[:, pl.ds(low, half)])
    up_out[...] = over_last(rows, up_ref[:, pl.ds(low, half)])


def store_blocks(ref, value):
    for j in range(N_BLK):
        ref[j] = value[:, LANES * j : LANES * (j + 1)].astype(BF16)


def down_columns(down_ref, parity):
    parts = []
    for j in range(N_BLK):
        low = pl.multiple_of((2 * j + parity) * LANES, LANES)
        parts.append(down_ref[:, pl.ds(low, LANES)])
    return jnp.concatenate(parts, axis=1)


def second_half_kernel(
    core_ref, other_ref, gate_ref, up_ref, down_ref, gate_in, up_in, hidden_out, out_ref
):
    half = gate_ref.shape[1] // 2
    other = 1 - core_ref[0]
    low = pl.multiple_of(other * half, half)
    rows = unpacked(other_ref)
    gate = gate_in[...] + over_last(rows, gate_ref[:, pl.ds(low, half)])
    up = up_in[...] + over_last(rows, up_ref[:, pl.ds(low, half)])
    hidden = (gate * jax.nn.sigmoid(gate) * up).astype(BF16)
    hidden_out[...] = hidden
    store_blocks(out_ref, dot(hidden, down_columns(down_ref, other)))


def own_down_kernel(core_ref, hidden_ref, down_ref, out_ref):
    store_blocks(out_ref, dot(hidden_ref[...], down_columns(down_ref, core_ref[0])))


def collect_kernel(parts_ref, out_ref):
    total = parts_ref[0].astype(F32)
    for j in range(1, N_BLK):
        total = total + parts_ref[j].astype(F32)
    total = total.astype(BF16)
    rows = N_EXP * HEAD_ROWS
    out_ref[:, :HEAD_ROWS, :] = total[:rows].reshape(N_EXP, HEAD_ROWS, LANES)
    shape = (N_EXP * 8, N_EXP * TAIL_ROWS)
    r, col = (iota(shape, 0), iota(shape, 1))
    spread = (r // 8 * TAIL_ROWS + r % 8 == col) & (r % 8 < TAIL_ROWS)
    tail = dot(spread.astype(BF16), total[rows:]).reshape(N_EXP, 8, LANES)
    out_ref[:, HEAD_ROWS:, :] = tail.astype(BF16)


def weights_kernel(routes_ref, logit_ref, out_ref):
    tokens = routes_ref.shape[0]
    routes = routes_ref[...]
    logit = logit_ref[...]
    expert = iota((tokens, N_EXP), 1)
    picks = [(routes[:, k : k + 1] == expert).astype(F32) for k in range(2)]
    before = (iota((tokens, tokens), 1) < iota((tokens, tokens), 0)).astype(BF16)
    ranks = dot(before, (picks[0] + picks[1]).astype(BF16))
    rows = N_EXP * HEAD_ROWS
    col = iota((tokens, rows + N_EXP * 8), 1)
    total = jnp.zeros(col.shape, F32)
    for k in range(2):
        weight = jax.nn.sigmoid(logit[:, k : k + 1] - logit[:, 1 - k : 2 - k])
        rank = jnp.sum(ranks * picks[k], axis=1, keepdims=True).astype(jnp.int32)
        route = routes[:, k : k + 1]
        place = jnp.where(
            rank < HEAD_ROWS,
            route * HEAD_ROWS + rank,
            rows + route * 8 + rank - HEAD_ROWS,
        )
        total = total + jnp.where(col == place, weight, 0.0)
    high = total.astype(BF16)
    out_ref[0] = high
    out_ref[1] = (total - high.astype(F32)).astype(BF16)


def combine_kernel(back_ref, weight_ref, out_ref):
    rows = N_EXP * HEAD_ROWS
    back = jnp.concatenate(
        [
            back_ref[:, :HEAD_ROWS, :].reshape(rows, LANES),
            back_ref[:, HEAD_ROWS:, :].reshape(N_EXP * 8, LANES),
        ],
        axis=0,
    )
    out_ref[...] = (dot(weight_ref[0], back) + dot(weight_ref[1], back)).astype(BF16)


def exchange(value, axes):
    return lax.all_to_all(value, axes, split_axis=0, concat_axis=0, tiled=True)


def from_behind(value, steps):
    count = lax.axis_size(EP)
    return lax.ppermute(value, EP, [(k, k + steps) for k in range(count - steps)])


def join(after, before):
    return call(join_kernel, sds(after.shape, BF16), (after, before), 10**8, vmem=4)


def swap_cores(value):
    return lax.ppermute(value, "c", [(0, 1), (1, 0)])


def dispatch(moe_rows, moe_gain, routes):
    core = lax.axis_index("c").astype(jnp.int32)[None]
    outbox = call(
        prep_kernel,
        sds((N_EXP, CHUNK, LANES), BF16),
        (core, moe_rows, moe_gain[None, :], routes.T),
        5 * 10**8,
        smem=1,
        hbm=3,
        scratch=(
            pltpu.VMEM(moe_rows.shape, BF16),
            pltpu.VMEM((1, moe_gain.shape[0]), F32),
            pltpu.VMEM(routes.shape[::-1], jnp.int32),
            pltpu.SemaphoreType.DMA((3,)),
        ),
    )
    return core, outbox


def run_experts(core, own, w_gate, w_up, w_down):
    rows, hidden_units = (N_EXP * CAP, w_gate.shape[2])
    gate, up, down = (w_gate[0].T, w_up[0].T, w_down[0])
    other = swap_cores(own)
    half_act = sds((rows, hidden_units), F32)
    gate_act, up_act = call(
        first_half_kernel, (half_act, half_act), (core, own, gate, up), 10**9, smem=1, vmem=20
    )
    packed = sds((N_BLK, rows, LANES), BF16)
    hidden, theirs = call(
        second_half_kernel,
        (sds((rows, hidden_units), BF16), packed),
        (core, other, gate, up, down, gate_act, up_act),
        2 * 10**9,
        smem=1,
        vmem=24,
    )
    arrived = swap_cores(theirs)
    mine = call(own_down_kernel, packed, (core, hidden, down), 6 * 10**8, smem=1, vmem=16)
    return (mine.astype(F32) + arrived.astype(F32)).astype(BF16)


def rim_kernel(group_ref, x_hbm, b_hbm, c_hbm, out_ref, x_ref, b_ref, c_ref, sems):
    low = pl.multiple_of(group_ref[0] * NSTATE, NSTATE)
    length = x_hbm.shape[1]
    last = pl.ds(length - LANES, LANES)
    fetch(
        (
            (x_hbm.at[:, last], x_ref),
            (b_hbm.at[pl.ds(low, NSTATE), last], b_ref),
            (c_hbm.at[pl.ds(low, NSTATE), last], c_ref),
        ),
        sems,
    )
    rows = jnp.concatenate([r[...].astype(F32) for r in (x_ref, b_ref, c_ref)], axis=0)
    out_ref[...] = rows.T[LANES - 8 :, :].astype(BF16)


def conv(signal, rim, taps):
    length = signal.shape[1]
    joined = jnp.concatenate([rim, signal], axis=1)
    total = taps[:, TAPS - 1 : TAPS] * signal
    for back in range(1, TAPS):
        moved = pltpu.roll(joined, back, axis=1)[:, LANES : LANES + length]
        total = total + taps[:, TAPS - 1 - back : TAPS - back] * moved
    return total * jax.nn.sigmoid(total)


def upright(taps):
    return jnp.concatenate([taps, jnp.zeros((4, taps.shape[1]), F32)], axis=0).T


def over_first(a, b):
    return lax.dot_general(a, b, (((0,), (0,)), ((), ())), preferred_element_type=F32)


def over_last(a, b):
    return lax.dot_general(a, b, (((1,), (1,)), ((), ())), preferred_element_type=F32)


def local_kernel(
    group_ref, x_hbm, b_hbm, c_hbm, rim_ref, dt_ref, rate_ref, tx_ref, tb_ref, tc_ref,
    x_out, b_out, c_out, cum_out, step_out, sent_out, x_ref, b_ref, c_ref, sems,
):
    heads, length = dt_ref.shape
    values = x_ref.shape[0]
    low = pl.multiple_of(group_ref[0] * NSTATE, NSTATE)
    own = pl.ds(low, NSTATE)
    fetch(((x_hbm, x_ref), (b_hbm.at[own], b_ref), (c_hbm.at[own], c_ref)), sems)
    rim = jnp.concatenate(
        [jnp.zeros((LANES - 8, values + 2 * NSTATE), F32), rim_ref[...].astype(F32)], axis=0
    ).T
    x = conv(x_ref[...].astype(F32), rim[:values], upright(tx_ref[...]))
    b_rim = rim[values : values + NSTATE]
    b = conv(b_ref[...].astype(F32), b_rim, upright(tb_ref[:, own])).astype(BF16)
    c_rim = rim[values + NSTATE :]
    c = conv(c_ref[...].astype(F32), c_rim, upright(tc_ref[:, own])).astype(BF16)
    raw = dt_ref[...]
    step = jnp.maximum(raw, 0.0) + jnp.log1p(jnp.exp(-jnp.abs(raw)))
    cum = -step * rate_ref[...]
    lane = iota((heads, length), 1)
    move = 1
    while move < length:
        cum = cum + jnp.where(lane >= move, pltpu.roll(cum, move, axis=1), 0.0)
        move *= 2
    x16 = x.astype(BF16)
    x_out[...] = x16
    b_out[...] = b
    c_out[...] = c
    cum_out[...] = cum
    step_out[...] = step
    end = cum[:, length - 1 : length]
    tail = jnp.exp(end - cum) * step
    sends = []
    for h in range(heads):
        rows = slice(HEAD_DIM * h, HEAD_DIM * (h + 1))
        weighted = (x[rows] * tail[h : h + 1]).astype(BF16)
        state = over_last(weighted, b)
        total = jnp.exp(end[h : h + 1])
        high = total.astype(BF16).astype(F32)
        sent_out[rows, :] = state.astype(BF16)
        sends += [high, total - high]
    sent_out[heads * HEAD_DIM :, :] = in_rows(sends).astype(BF16)


def in_rows(values):
    row = iota((16, LANES), 0)
    total = jnp.zeros((16, LANES), F32)
    for k, value in enumerate(values):
        total = jnp.where(row == k, value, total)
    return total


def inner_kernel(x_ref, b_ref, c_ref, cum_ref, step_ref, y_out):
    heads, length = cum_ref.shape
    cum = cum_ref[...]
    pad = jnp.zeros((LANES - 2 * heads, length), F32)
    columns = jnp.concatenate([cum, step_ref[...], pad], axis=0).T
    score = over_first(b_ref[...], c_ref[...])
    for h in range(heads):
        rows = slice(HEAD_DIM * h, HEAD_DIM * (h + 1))
        for t in range(length // LANES):
            here = slice(LANES * t, LANES * (t + 1))
            size = LANES * (t + 1)
            gap = cum[h : h + 1, here] - columns[:size, h : h + 1]
            inside = iota((size, LANES), 0) <= iota((size, LANES), 1) + LANES * t
            decay = jnp.exp(jnp.where(inside, gap, -1e30))
            mask = score[:size, here] * decay * columns[:size, heads + h : heads + h + 1]
            y_out[rows, here] = dot(x_ref[rows, :size], mask.astype(BF16))


def join_kernel(after_ref, before_ref, out_ref):
    size = after_ref.shape[0] - 16
    after = after_ref[...].astype(F32)
    before = before_ref[...].astype(F32)
    decays = []
    for h in range(size // HEAD_DIM):
        rows = slice(HEAD_DIM * h, HEAD_DIM * (h + 1))
        pair = slice(size + 2 * h, size + 2 * h + 1)
        rest = slice(size + 2 * h + 1, size + 2 * h + 2)
        own = after[pair] + after[rest]
        out_ref[rows, :] = (after[rows] + own * before[rows]).astype(BF16)
        total = own * (before[pair] + before[rest])
        high = total.astype(BF16).astype(F32)
        decays += [high, total - high]
    out_ref[size:, :] = in_rows(decays).astype(BF16)


def mixed_kernel(y_ref, before_ref, c_ref, cum_ref, z_ref, gain_ref, out_ref):
    heads = cum_ref.shape[0]
    reach = jnp.exp(cum_ref[...])
    carried = dot(before_ref[: heads * HEAD_DIM, :], c_ref[...])
    for h in range(heads):
        rows = slice(HEAD_DIM * h, HEAD_DIM * (h + 1))
        z = z_ref[rows, :].astype(F32)
        y = y_ref[rows, :] + carried[rows] * reach[h : h + 1]
        gated = y * (z * jax.nn.sigmoid(z))
        scale = lax.rsqrt(jnp.mean(gated * gated, axis=0, keepdims=True) + HEAD_EPS)
        out_ref[rows, :] = (gated * scale * gain_ref[rows, :]).astype(BF16)


def rims_of(group, x_in, b_in, c_in):
    rows = x_in.shape[0] + 2 * NSTATE
    own = call(
        rim_kernel,
        sds((8, rows), BF16),
        (group, x_in, b_in, c_in),
        10**8,
        smem=1,
        hbm=3,
        vmem=4,
        scratch=(
            pltpu.VMEM((x_in.shape[0], LANES), BF16),
            pltpu.VMEM((NSTATE, LANES), BF16),
            pltpu.VMEM((NSTATE, LANES), BF16),
            pltpu.SemaphoreType.DMA((3,)),
        ),
    )
    return from_behind(own, 1)


def on_device(
    x_in,
    z_in,
    dt_raw,
    decay_rate,
    b_in,
    c_in,
    conv_x,
    conv_b,
    conv_c,
    head_gain,
    moe_rows,
    moe_gain,
    routes,
    route_logit,
    w_gate,
    w_up,
    w_down,
):
    heads, length = dt_raw.shape
    values = x_in.shape[0]
    core, outbox = dispatch(moe_rows, moe_gain, routes)
    group = lax.axis_index(TP) * heads // (HEADS // GROUPS)
    group = group.astype(jnp.int32)[None]
    rims = rims_of(group, x_in, b_in, c_in)
    arrived = exchange(outbox, EP)
    x_conv, b_conv, c_conv, cum, step_dt, sent = call(
        local_kernel,
        (
            sds((values, length), BF16),
            sds((NSTATE, length), BF16),
            sds((NSTATE, length), BF16),
            sds((heads, length), F32),
            sds((heads, length), F32),
            sds((values + 16, LANES), BF16),
        ),
        (
            group, x_in, b_in, c_in, rims, dt_raw, decay_rate[:, None],
            conv_x.T, conv_b.T, conv_c.T,
        ),
        2 * 10**9,
        smem=1,
        hbm=3,
        scratch=(
            pltpu.VMEM((values, length), BF16),
            pltpu.VMEM((NSTATE, length), BF16),
            pltpu.VMEM((NSTATE, length), BF16),
            pltpu.SemaphoreType.DMA((3,)),
        ),
    )
    nearest = from_behind(sent, 1)
    second = from_behind(sent, 2)
    y_local = call(
        inner_kernel,
        sds((values, length), F32),
        (x_conv, b_conv, c_conv, cum, step_dt),
        2 * 10**9,
    )
    spans = join(nearest, second)
    for steps in (2, 4, 8, 16):
        behind = from_behind(spans, steps)
        spans = join(spans, behind)
    weights = call(
        weights_kernel,
        sds((2, moe_rows.shape[0], N_EXP * (HEAD_ROWS + 8)), BF16),
        (routes, route_logit),
        10**9,
    )
    partial = run_experts(core, arrived, w_gate, w_up, w_down)
    parts = exchange(partial, "y")
    collected = call(
        collect_kernel, sds((N_EXP, HEAD_ROWS + 8, LANES), BF16), (parts,), 10**8
    )
    back = exchange(collected, EP)
    mixed = call(
        mixed_kernel,
        sds((values, length), BF16),
        (y_local, spans, c_conv, cum, z_in, head_gain[:, None]),
        2 * 10**9,
    )
    moe_out = call(
        combine_kernel, sds((moe_rows.shape[0], LANES), BF16), (back, weights), 10**8
    ).T
    return (mixed, moe_out)


def solution(mesh):
    finer = Mesh(mesh.devices.reshape(8, 4, 8, 2), ("z", "x", "y", "c"))
    in_specs = (
        P(TP, EP),
        P(TP, EP),
        P(TP, EP),
        P(TP),
        P(None, EP),
        P(None, EP),
        P(TP, None),
        P(),
        P(),
        P(TP),
        P(EP, None),
        P(),
        P(EP, None),
        P(EP, None),
        P(EP, None, TP),
        P(EP, None, TP),
        P(EP, TP, None),
    )
    out_specs = (P(TP, EP), P(TP, EP))

    return jax.shard_map(
        on_device, mesh=finer, in_specs=in_specs, out_specs=out_specs, check_vma=False
    )
```

time: 195 us -> 145 us (0.74)
  the two profiles are of different devices: /device:TPU:24 before, /device:TPU:8 now
where the time goes in v1:
time: 145 us; the launch traced here: 144 us
  starting transfers between devices  56.8 us (39%)
  blocking collectives  48.3 us (33%)
  waiting for transfers between devices  20.4 us (14%)
  Pallas kernels  13.3 us (9%)
  local copies, waits for them, and re-layouts  3 us (2%)
    all_to_all x1, blocking collectives, exchange(): return lax.all_to_all(value, axes, split_axis=0, concat_axis=0, tiled=True)  48.3 us
    ppermute x7, starting transfers between devices, from_behind(): lax.ppermute(value, EP, [(k, k + steps) for k in range(count - steps)])  41.3 us
    pallas_call x16, Pallas kernels, call(): pl.pallas_call(kernel, out_shape=out_shape, in_specs=specs, out_specs=jax...  13.3 us
    all_to_all x2, starting transfers between devices, exchange(): return lax.all_to_all(value, axes, split_axis=0, concat_axis=0, tiled=True)  11.6 us
    all_to_all x2, waiting for transfers between devices, exchange(): return lax.all_to_all(value, axes, split_axis=0, concat_axis=0, tiled=True)  9.22 us
    ppermute x7, waiting for transfers between devices, from_behind(): lax.ppermute(value, EP, [(k, k + steps) for k in range(count - steps)])  7.94 us
    ppermute x2, starting transfers between devices, swap_cores(): return lax.ppermute(value, 'c', [(0, 1), (1, 0)])  3.95 us
    ppermute x2, waiting for transfers between devices, swap_cores(): return lax.ppermute(value, 'c', [(0, 1), (1, 0)])  3.19 us
  transfers between devices with their start and end apart: 11, of which 8 were waited for; matrix products, arithmetic and copies ran while one was open for 0% of the time, Pallas kernels for 6%

profile of v1, /device:TPU:8, one launch (start us, length us, event | category | flops | bytes accessed | tf_op | source)
XLA Modules:
  0.0 144.3 jit_solution(11708215396567143340)
XLA Ops:
  0.6 0.0 copy-start.3
  0.6 1.1 copy-done.3
  1.7 0.7 copy-done.7
  2.4 0.7 copy-done.8
  3.1 1.3 shard_map.185
  4.4 0.0 copy-start.1
  4.4 0.0 copy-start.2
  4.4 48.3 %all_to_all.15.own_ref = bf16[32,160,128]{2,1,0:T(8,128)(2,1)S(1)} all-to-all(bf16[32,160,128]{2,1,0:T(8,128)(2,1)S(1)} %shard_map.185), channel_id=1, replica_groups=mesh['z'=8,'x'=4,'y'=8,'c'=2] {'z','x'}, dimensions={0} | all-to-all | bytes 2621440 | tf_op jit(solution)/shard_map/all_to_all | solution.py:251
  52.8 1.9 %collective-permute-start.7 = (bf16[32,160,128]{2,1,0:T(8,128)(2,1)S(1)}, bf16[32,160,128]{2,1,0:T(8,128)(2,1)S(1)}, u32[]{:S(2)}, u32[]{:S(2)}) collective-permute-start(bf16[32,160,128]{2,1,0:T(8,128)(2,1)S(1)} %all_to_all.15.own_ref), channel_id=1, source_target_pairs={{0,1},{1,0},{2,3},{3,2},{4,5},{5,4},{6,7},{7,6},{8,9},{9,8},{10,11... | collective-permute-start | bytes 3932168 | tf_op jit(solution)/shard_map/ppermute | solution.py:264
  54.7 0.0 copy-done.1
  54.7 0.0 copy-done.2
  54.7 0.0 copy-start
  54.7 1.7 %shard_map.186 = (f32[640,320]{1,0:T(8,128)S(1)}, f32[640,320]{1,0:T(8,128)S(1)}) custom-call(s32[1]{0:T(128)} %bitcast.6.core_ref, bf16[32,160,128]{2,1,0:T(8,128)(2,1)S(1)} %all_to_all.15.own_ref, bf16[320,2048]{1,0:T(8,128)(2,1)S(1)} %bitcast.19, bf16[320,2048]{1,0:T(8,128)(2,1)S(1)} %bitcast.21), custom_call_target="tpu_custom_call" | custom-call | flops 1000000000 | bytes 1048576 | tf_op jit(solution)/shard_map/pallas_call | solution.py:44
  56.5 1.2 collective-permute-done.7.other_ref
  57.7 0.0 copy-done
  57.7 2.6 %shard_map.187 = (bf16[640,320]{1,0:T(8,128)(2,1)S(1)}, bf16[8,640,128]{2,1,0:T(8,128)(2,1)S(1)}) custom-call(s32[1]{0:T(128)} %bitcast.6.core_ref, bf16[32,160,128]{2,1,0:T(8,128)(2,1)S(1)} %collective-permute-done.7.other_ref, bf16[320,2048]{1,0:T(8,128)(2,1)S(1)} %bitcast.20, bf16[320,2048]{1,0:T(8,128)(2,1)S(1)} %bitcast.22, ...), custom_call_target="tpu_custom_call" | custom-call | flops 2000000000 | bytes 1048576 | tf_op jit(solution)/shard_map/pallas_call | solution.py:44
  60.3 2.0 %collective-permute-start.8 = (bf16[8,640,128]{2,1,0:T(8,128)(2,1)S(1)}, bf16[8,640,128]{2,1,0:T(8,128)(2,1)S(1)}, u32[]{:S(2)}, u32[]{:S(2)}) collective-permute-start(bf16[8,640,128]{2,1,0:T(8,128)(2,1)S(1)} %get-tuple-element.21), channel_id=1, source_target_pairs={{0,1},{1,0},{2,3},{3,2},{4,5},{5,4},{6,7},{7,6},{8,9},{9,8},{10,11... | collective-permute-start | bytes 3932168 | tf_op jit(solution)/shard_map/ppermute | solution.py:264
  62.3 0.9 shard_map.188
  63.2 2.0 %collective-permute-done.8 = bf16[8,640,128]{2,1,0:T(8,128)(2,1)S(1)} collective-permute-done((bf16[8,640,128]{2,1,0:T(8,128)(2,1)S(1)}, bf16[8,640,128]{2,1,0:T(8,128)(2,1)S(1)}, u32[]{:S(2)}, u32[]{:S(2)}) %collective-permute-start.8) | collective-permute-done | bytes 1310752 | tf_op jit(solution)/shard_map/ppermute | solution.py:264
  65.2 1.4 add_convert_fusion
  66.6 0.0 copy-start.11
  66.6 0.0 copy-start.12
  66.7 0.0 copy-start.13
  66.7 0.0 copy-start.14
  66.7 7.7 %all-to-all-start.1 = ((bf16[8,640,128]{2,1,0:T(8,128)(2,1)}), bf16[8,640,128]{2,1,0:T(8,128)(2,1)S(1)}, u32[]{:S(2)}, u32[]{:S(2)}) async-start(bf16[8,640,128]{2,1,0:T(8,128)(2,1)} %add_convert_fusion), calls=%async_computation.1 | async-start | bytes 2621440 | tf_op jit(solution)/shard_map/all_to_all | solution.py:251
  74.4 0.0 copy-done.4
  74.4 0.0 copy-done.5
  74.4 0.0 copy-done.6
  74.4 0.2 shard_map.176
  74.6 2.1 %collective-permute-start = (bf16[8,512]{1,0:T(8,128)(2,1)S(1)}, bf16[8,512]{1,0:T(8,128)(2,1)S(1)}, u32[]{:S(2)}, u32[]{:S(2)}) collective-permute-start(bf16[8,512]{1,0:T(8,128)(2,1)S(1)} %shard_map.176), channel_id=1, source_target_pairs={{0,16},{16,32},{32,48},{48,64},{64,80},{80,96},{96,112},{112,128},... | collective-permute-start | bytes 24584 | tf_op jit(solution)/shard_map/ppermute | solution.py:256
  76.7 0.0 copy-done.17
  76.7 0.1 copy.22.rate_ref
  76.8 1.2 collective-permute-done.rim_ref
  78.1 0.0 copy-done.11
  78.1 0.0 copy-done.13
  78.1 0.0 copy-start.9
  78.1 0.0 copy-start.16
  78.1 0.0 copy-start.15
  78.1 2.2 %shard_map.177 = (bf16[256,384]{1,0:T(8,128)(2,1)S(1)}, bf16[128,384]{1,0:T(8,128)(2,1)S(1)}, bf16[128,384]{1,0:T(8,128)(2,1)S(1)}, f32[4,384]{1,0:T(4,128)S(1)}...) custom-call(s32[1]{0:T(128)} %bitcast.group_ref, bf16[256,384]{1,0:T(8,128)(2,1)S(1)} %copy-done.4, ...), custom_call_target="tpu_custom_call" | custom-call | flops 2000000000 | bytes 1048576 | tf_op jit(solution)/shard_map/pallas_call | solution.py:44
  80.3 4.2 %collective-permute-start.1 = (bf16[272,128]{1,0:T(8,128)(2,1)S(1)}, bf16[272,128]{1,0:T(8,128)(2,1)S(1)}, u32[]{:S(2)}, u32[]{:S(2)}) collective-permute-start(bf16[272,128]{1,0:T(8,128)(2,1)S(1)} %get-tuple-element.17), channel_id=1, source_target_pairs={{0,16},{16,32},{32,48},{48,64},{64,80},{80,96},{96,112},{112,128},... | collective-permute-start | bytes 208904 | tf_op jit(solution)/shard_map/ppermute | solution.py:256
  84.5 4.7 %collective-permute-start.2 = (bf16[272,128]{1,0:T(8,128)(2,1)S(1)}, bf16[272,128]{1,0:T(8,128)(2,1)S(1)}, u32[]{:S(2)}, u32[]{:S(2)}) collective-permute-start(bf16[272,128]{1,0:T(8,128)(2,1)S(1)} %get-tuple-element.17), channel_id=1, source_target_pairs={{0,32},{16,48},{32,64},{48,80},{64,96},{80,112},{96,128},{112,144}... | collective-permute-start | bytes 208904 | tf_op jit(solution)/shard_map/ppermute | solution.py:256
  89.2 0.0 collective-permute-done.1.after_ref
  89.2 1.9 %collective-permute-done.2.before_ref = bf16[272,128]{1,0:T(8,128)(2,1)S(1)} collective-permute-done((bf16[272,128]{1,0:T(8,128)(2,1)S(1)}, bf16[272,128]{1,0:T(8,128)(2,1)S(1)}, u32[]{:S(2)}, u32[]{:S(2)}) %collective-permute-start.2) | collective-permute-done | bytes 69664 | tf_op jit(solution)/shard_map/ppermute | solution.py:256
  91.2 5.8 %collective-permute-start.3 = (bf16[272,128]{1,0:T(8,128)(2,1)S(1)}, bf16[272,128]{1,0:T(8,128)(2,1)S(1)}, u32[]{:S(2)}, u32[]{:S(2)}) collective-permute-start(bf16[272,128]{1,0:T(8,128)(2,1)S(1)} %shard_map.179.after_ref), channel_id=1, source_target_pairs={{0,32},{16,48},{32,64},{48,80},{64,96},{80,112},{96,128},{112,144}... | collective-permute-start | bytes 208904 | tf_op jit(solution)/shard_map/ppermute | solution.py:256
  96.9 1.9 %collective-permute-done.3.before_ref = bf16[272,128]{1,0:T(8,128)(2,1)S(1)} collective-permute-done((bf16[272,128]{1,0:T(8,128)(2,1)S(1)}, bf16[272,128]{1,0:T(8,128)(2,1)S(1)}, u32[]{:S(2)}, u32[]{:S(2)}) %collective-permute-start.3) | collective-permute-done | bytes 69664 | tf_op jit(solution)/shard_map/ppermute | solution.py:256
  98.9 7.9 %collective-permute-start.4 = (bf16[272,128]{1,0:T(8,128)(2,1)S(1)}, bf16[272,128]{1,0:T(8,128)(2,1)S(1)}, u32[]{:S(2)}, u32[]{:S(2)}) collective-permute-start(bf16[272,128]{1,0:T(8,128)(2,1)S(1)} %shard_map.180.after_ref), channel_id=1, source_target_pairs={{0,64},{16,80},{32,96},{48,112},{64,128},{80,144},{96,160},{112,17... | collective-permute-start | bytes 208904 | tf_op jit(solution)/shard_map/ppermute | solution.py:256
  106.8 0.1 copy.24.routes_ref
  106.9 0.1 copy.23.gain_ref
  107.1 0.1 copy.25.logit_ref
  107.2 1.5 %collective-permute-done.4.before_ref = bf16[272,128]{1,0:T(8,128)(2,1)S(1)} collective-permute-done((bf16[272,128]{1,0:T(8,128)(2,1)S(1)}, bf16[272,128]{1,0:T(8,128)(2,1)S(1)}, u32[]{:S(2)}, u32[]{:S(2)}) %collective-permute-start.4) | collective-permute-done | bytes 69664 | tf_op jit(solution)/shard_map/ppermute | solution.py:256
  108.7 4.4 %collective-permute-start.5 = (bf16[272,128]{1,0:T(8,128)(2,1)S(1)}, bf16[272,128]{1,0:T(8,128)(2,1)S(1)}, u32[]{:S(2)}, u32[]{:S(2)}) collective-permute-start(bf16[272,128]{1,0:T(8,128)(2,1)S(1)} %shard_map.181.after_ref), channel_id=1, source_target_pairs={{0,128},{16,144},{32,160},{48,176},{64,192},{80,208},{96,224},{112... | collective-permute-start | bytes 208904 | tf_op jit(solution)/shard_map/ppermute | solution.py:256
  113.1 0.6 shard_map.190.weight_ref
  113.7 1.3 collective-permute-done.5.before_ref
  115.1 12.3 %collective-permute-start.6 = (bf16[272,128]{1,0:T(8,128)(2,1)S(1)}, bf16[272,128]{1,0:T(8,128)(2,1)S(1)}, u32[]{:S(2)}, u32[]{:S(2)}) collective-permute-start(bf16[272,128]{1,0:T(8,128)(2,1)S(1)} %shard_map.182.after_ref), channel_id=1, source_target_pairs={{0,256},{16,272},{32,288},{48,304},{64,320},{80,336},{96,352},{112... | collective-permute-start | bytes 208904 | tf_op jit(solution)/shard_map/ppermute | solution.py:256
  127.4 0.0 all-to-all-done.1.parts_ref
  127.4 1.0 shard_map.189
  128.4 3.9 %all-to-all-start.2 = ((bf16[32,24,128]{2,1,0:T(8,128)(2,1)}), bf16[32,24,128]{2,1,0:T(8,128)(2,1)S(1)}, u32[]{:S(2)}, u32[]{:S(2)}) async-start(bf16[32,24,128]{2,1,0:T(8,128)(2,1)} %shard_map.189), calls=%async_computation.2 | async-start | bytes 393216 | tf_op jit(solution)/shard_map/all_to_all | solution.py:251
  132.2 0.0 copy-start.10
  132.3 0.8 shard_map.178.y_ref
  133.1 0.0 collective-permute-done.6.before_ref
  133.2 0.0 copy-done.10
  133.2 1.0 shard_map.184
  134.2 9.2 %all-to-all-done.2.back_ref = bf16[32,24,128]{2,1,0:T(8,128)(2,1)S(1)} async-done(((bf16[32,24,128]{2,1,0:T(8,128)(2,1)}), bf16[32,24,128]{2,1,0:T(8,128)(2,1)S(1)}, u32[]{:S(2)}, u32[]{:S(2)}) %all-to-all-start.2) | async-done | bytes 196640 | tf_op jit(solution)/shard_map/all_to_all | solution.py:251
  143.4 0.9 shard_map.191
  (16 shorter events, 0.2 us)
Async XLA Ops:
  0.6 1.1 copy-start.3
  1.7 0.7 copy-start.7
  2.4 0.7 copy-start.8
  4.4 50.3 %copy-start.1 = (bf16[1,2048,320]{1,2,0:T(8,128)(2,1)S(1)}, bf16[1,2048,320]{1,2,0:T(8,128)(2,1)}, u32[]{:S(2)}) copy-start(bf16[1,2048,320]{1,2,0:T(8,128)(2,1)} %param.31) | copy-start | bytes 3932164
  4.4 50.3 %copy-start.2 = (bf16[1,2048,320]{1,2,0:T(8,128)(2,1)S(1)}, bf16[1,2048,320]{1,2,0:T(8,128)(2,1)}, u32[]{:S(2)}) copy-start(bf16[1,2048,320]{1,2,0:T(8,128)(2,1)} %param.32) | copy-start | bytes 3932164
  52.8 4.9 %collective-permute-start.7 = (bf16[32,160,128]{2,1,0:T(8,128)(2,1)S(1)}, bf16[32,160,128]{2,1,0:T(8,128)(2,1)S(1)}, u32[]{:S(2)}, u32[]{:S(2)}) collective-permute-start(bf16[32,160,128]{2,1,0:T(8,128)(2,1)S(1)} %all_to_all.15.own_ref), channel_id=1, source_target_pairs={{0,1},{1,0},{2,3},{3,2},{4,5},{5,4},{6,7},{7,6},{8,9},{9,8},{10,11... | collective-permute-start | bytes 3932168 | tf_op jit(solution)/shard_map/ppermute | solution.py:264
  54.7 3.0 %copy-start = (bf16[1,320,2048]{2,1,0:T(8,128)(2,1)S(1)}, bf16[1,320,2048]{2,1,0:T(8,128)(2,1)}, u32[]{:S(2)}) copy-start(bf16[1,320,2048]{2,1,0:T(8,128)(2,1)} %param.33) | copy-start | bytes 3932164
  60.3 4.9 %collective-permute-start.8 = (bf16[8,640,128]{2,1,0:T(8,128)(2,1)S(1)}, bf16[8,640,128]{2,1,0:T(8,128)(2,1)S(1)}, u32[]{:S(2)}, u32[]{:S(2)}) collective-permute-start(bf16[8,640,128]{2,1,0:T(8,128)(2,1)S(1)} %get-tuple-element.21), channel_id=1, source_target_pairs={{0,1},{1,0},{2,3},{3,2},{4,5},{5,4},{6,7},{7,6},{8,9},{9,8},{10,11... | collective-permute-start | bytes 3932168 | tf_op jit(solution)/shard_map/ppermute | solution.py:264
  66.6 7.8 %copy-start.4 = (bf16[256,384]{1,0:T(8,128)(2,1)S(1)}, bf16[256,384]{1,0:T(8,128)(2,1)}, u32[]{:S(2)}) copy-start(bf16[256,384]{1,0:T(8,128)(2,1)} %x_hbm.3) | copy-start | bytes 589828
  66.6 7.8 %copy-start.5 = (bf16[256,384]{1,0:T(8,128)(2,1)S(1)}, bf16[256,384]{1,0:T(8,128)(2,1)}, u32[]{:S(2)}) copy-start(bf16[256,384]{1,0:T(8,128)(2,1)} %b_hbm.3) | copy-start | bytes 589828
  66.6 7.8 %copy-start.6 = (bf16[256,384]{1,0:T(8,128)(2,1)S(1)}, bf16[256,384]{1,0:T(8,128)(2,1)}, u32[]{:S(2)}) copy-start(bf16[256,384]{1,0:T(8,128)(2,1)} %c_hbm.3) | copy-start | bytes 589828
  66.6 10.1 %copy-start.17 = (f32[4]{0:T(128)S(1)}, f32[4]{0:T(128)}, u32[]{:S(2)}) copy-start(f32[4]{0:T(128)} %param.20) | copy-start | bytes 52
  66.6 11.4 %copy-start.11 = (f32[4,384]{1,0:T(4,128)S(1)}, f32[4,384]{1,0:T(4,128)}, u32[]{:S(2)}) copy-start(f32[4,384]{1,0:T(4,128)} %dt_ref.1) | copy-start | bytes 18436
  66.6 11.4 %copy-start.12 = (f32[256,4]{0,1:T(4,128)S(1)}, f32[256,4]{0,1:T(4,128)}, u32[]{:S(2)}) copy-start(f32[256,4]{0,1:T(4,128)} %param.23) | copy-start | bytes 12292
  66.7 11.4 %copy-start.13 = (f32[256,4]{0,1:T(4,128)S(1)}, f32[256,4]{0,1:T(4,128)}, u32[]{:S(2)}) copy-start(f32[256,4]{0,1:T(4,128)} %param.24) | copy-start | bytes 12292
  66.7 11.4 %copy-start.14 = (f32[256,4]{0,1:T(4,128)S(1)}, f32[256,4]{0,1:T(4,128)}, u32[]{:S(2)}) copy-start(f32[256,4]{0,1:T(4,128)} %param.25) | copy-start | bytes 12292
  66.7 60.7 %all-to-all-start.1 = ((bf16[8,640,128]{2,1,0:T(8,128)(2,1)}), bf16[8,640,128]{2,1,0:T(8,128)(2,1)S(1)}, u32[]{:S(2)}, u32[]{:S(2)}) async-start(bf16[8,640,128]{2,1,0:T(8,128)(2,1)} %add_convert_fusion), calls=%async_computation.1 | async-start | bytes 2621440 | tf_op jit(solution)/shard_map/all_to_all | solution.py:251
  74.6 3.5 %collective-permute-start = (bf16[8,512]{1,0:T(8,128)(2,1)S(1)}, bf16[8,512]{1,0:T(8,128)(2,1)S(1)}, u32[]{:S(2)}, u32[]{:S(2)}) collective-permute-start(bf16[8,512]{1,0:T(8,128)(2,1)S(1)} %shard_map.176), channel_id=1, source_target_pairs={{0,16},{16,32},{32,48},{48,64},{64,80},{80,96},{96,112},{112,128},... | collective-permute-start | bytes 24584 | tf_op jit(solution)/shard_map/ppermute | solution.py:256
  78.1 28.7 %copy-start.9 = (s32[160,2]{0,1:T(2,128)S(1)}, s32[160,2]{0,1:T(2,128)}, u32[]{:S(2)}) copy-start(s32[160,2]{0,1:T(2,128)} %param.29) | copy-start | bytes 3844
  78.1 28.8 %copy-start.16 = (f32[256]{0:T(256)S(1)}, f32[256]{0:T(256)}, u32[]{:S(2)}) copy-start(f32[256]{0:T(256)} %param.26) | copy-start | bytes 3076
  78.1 28.9 %copy-start.15 = (f32[160,2]{0,1:T(2,128)S(1)}, f32[160,2]{0,1:T(2,128)}, u32[]{:S(2)}) copy-start(f32[160,2]{0,1:T(2,128)} %param.30) | copy-start | bytes 3844
  80.3 8.9 %collective-permute-start.1 = (bf16[272,128]{1,0:T(8,128)(2,1)S(1)}, bf16[272,128]{1,0:T(8,128)(2,1)S(1)}, u32[]{:S(2)}, u32[]{:S(2)}) collective-permute-start(bf16[272,128]{1,0:T(8,128)(2,1)S(1)} %get-tuple-element.17), channel_id=1, source_target_pairs={{0,16},{16,32},{32,48},{48,64},{64,80},{80,96},{96,112},{112,128},... | collective-permute-start | bytes 208904 | tf_op jit(solution)/shard_map/ppermute | solution.py:256
  84.5 6.6 %collective-permute-start.2 = (bf16[272,128]{1,0:T(8,128)(2,1)S(1)}, bf16[272,128]{1,0:T(8,128)(2,1)S(1)}, u32[]{:S(2)}, u32[]{:S(2)}) collective-permute-start(bf16[272,128]{1,0:T(8,128)(2,1)S(1)} %get-tuple-element.17), channel_id=1, source_target_pairs={{0,32},{16,48},{32,64},{48,80},{64,96},{80,112},{96,128},{112,144}... | collective-permute-start | bytes 208904 | tf_op jit(solution)/shard_map/ppermute | solution.py:256
  91.2 7.7 %collective-permute-start.3 = (bf16[272,128]{1,0:T(8,128)(2,1)S(1)}, bf16[272,128]{1,0:T(8,128)(2,1)S(1)}, u32[]{:S(2)}, u32[]{:S(2)}) collective-permute-start(bf16[272,128]{1,0:T(8,128)(2,1)S(1)} %shard_map.179.after_ref), channel_id=1, source_target_pairs={{0,32},{16,48},{32,64},{48,80},{64,96},{80,112},{96,128},{112,144}... | collective-permute-start | bytes 208904 | tf_op jit(solution)/shard_map/ppermute | solution.py:256
  98.9 9.8 %collective-permute-start.4 = (bf16[272,128]{1,0:T(8,128)(2,1)S(1)}, bf16[272,128]{1,0:T(8,128)(2,1)S(1)}, u32[]{:S(2)}, u32[]{:S(2)}) collective-permute-start(bf16[272,128]{1,0:T(8,128)(2,1)S(1)} %shard_map.180.after_ref), channel_id=1, source_target_pairs={{0,64},{16,80},{32,96},{48,112},{64,128},{80,144},{96,160},{112,17... | collective-permute-start | bytes 208904 | tf_op jit(solution)/shard_map/ppermute | solution.py:256
  108.7 6.3 %collective-permute-start.5 = (bf16[272,128]{1,0:T(8,128)(2,1)S(1)}, bf16[272,128]{1,0:T(8,128)(2,1)S(1)}, u32[]{:S(2)}, u32[]{:S(2)}) collective-permute-start(bf16[272,128]{1,0:T(8,128)(2,1)S(1)} %shard_map.181.after_ref), channel_id=1, source_target_pairs={{0,128},{16,144},{32,160},{48,176},{64,192},{80,208},{96,224},{112... | collective-permute-start | bytes 208904 | tf_op jit(solution)/shard_map/ppermute | solution.py:256
  115.1 18.0 %collective-permute-start.6 = (bf16[272,128]{1,0:T(8,128)(2,1)S(1)}, bf16[272,128]{1,0:T(8,128)(2,1)S(1)}, u32[]{:S(2)}, u32[]{:S(2)}) collective-permute-start(bf16[272,128]{1,0:T(8,128)(2,1)S(1)} %shard_map.182.after_ref), channel_id=1, source_target_pairs={{0,256},{16,272},{32,288},{48,304},{64,320},{80,336},{96,352},{112... | collective-permute-start | bytes 208904 | tf_op jit(solution)/shard_map/ppermute | solution.py:256
  128.4 15.0 %all-to-all-start.2 = ((bf16[32,24,128]{2,1,0:T(8,128)(2,1)}), bf16[32,24,128]{2,1,0:T(8,128)(2,1)S(1)}, u32[]{:S(2)}, u32[]{:S(2)}) async-start(bf16[32,24,128]{2,1,0:T(8,128)(2,1)} %shard_map.189), calls=%async_computation.2 | async-start | bytes 393216 | tf_op jit(solution)/shard_map/all_to_all | solution.py:251
  132.2 0.9 copy-start.10

commit v2 on v1

--- a/solution.py
+++ b/solution.py
@@ -269,7 +269,13 @@
     outbox = call(
         prep_kernel,
         sds((N_EXP, CHUNK, LANES), BF16),
-        (core, moe_rows, moe_gain[None, :], routes.T),
+        (
+            core,
+            *(
+                pltpu.with_memory_space_constraint(a, pltpu.HBM)
+                for a in (moe_rows, moe_gain[None, :], routes.T)
+            ),
+        ),
         5 * 10**8,
         smem=1,
         hbm=3,
@@ -488,8 +494,8 @@
     core, outbox = dispatch(moe_rows, moe_gain, routes)
     group = lax.axis_index(TP) * heads // (HEADS // GROUPS)
     group = group.astype(jnp.int32)[None]
+    arrived = exchange(outbox, EP)
     rims = rims_of(group, x_in, b_in, c_in)
-    arrived = exchange(outbox, EP)
     x_conv, b_conv, c_conv, cum, step_dt, sent = call(
         local_kernel,
         (

time: 145 us -> 143 us (0.986)
  local copies, waits for them, and re-layouts: 3 us -> 0.54 us
    unnamed x38 -> x32, local copies, waits for them, and re-layouts: 2.77 us -> 0.31 us
where the time goes in v2:
time: 143 us
  starting transfers between devices  56.8 us (40%)
  blocking collectives  48.3 us (34%)
  waiting for transfers between devices  20.4 us (14%)
  Pallas kernels  14.2 us (10%)
  other arithmetic  1.44 us (1%)
    all_to_all x1, blocking collectives, exchange(): return lax.all_to_all(value, axes, split_axis=0, concat_axis=0, tiled=True)  48.3 us
    ppermute x7, starting transfers between devices, from_behind(): lax.ppermute(value, EP, [(k, k + steps) for k in range(count - steps)])  41.3 us
    pallas_call x16, Pallas kernels, call(): pl.pallas_call(kernel, out_shape=out_shape, in_specs=specs, out_specs=jax...  14.2 us
    all_to_all x2, starting transfers between devices, exchange(): return lax.all_to_all(value, axes, split_axis=0, concat_axis=0, tiled=True)  11.6 us
    all_to_all x2, waiting for transfers between devices, exchange(): return lax.all_to_all(value, axes, split_axis=0, concat_axis=0, tiled=True)  9.22 us
    ppermute x7, waiting for transfers between devices, from_behind(): lax.ppermute(value, EP, [(k, k + steps) for k in range(count - steps)])  7.94 us
    ppermute x2, starting transfers between devices, swap_cores(): return lax.ppermute(value, 'c', [(0, 1), (1, 0)])  3.95 us
    ppermute x2, waiting for transfers between devices, swap_cores(): return lax.ppermute(value, 'c', [(0, 1), (1, 0)])  3.19 us
  transfers between devices with their start and end apart: 11, of which 8 were waited for; matrix products, arithmetic and copies ran while one was open for 0% of the time, Pallas kernels for 6%

profile of v2, /device:TPU:8, one launch (start us, length us, event | category | flops | bytes accessed | tf_op | source)
XLA Modules:
  0.0 142.7 jit_solution(10986233720822689102)
XLA Ops:
  0.6 2.2 %shard_map.185 = bf16[32,160,128]{2,1,0:T(8,128)(2,1)S(1)} custom-call(s32[1]{0:T(128)} %bitcast.6.core_ref, bf16[160,2048]{1,0:T(8,128)(2,1)} %rows_hbm.1, f32[1,2048]{1,0:T(1,128)} %bitcast.27, s32[2,160]{1,0:T(2,128)} %bitcast.28), custom_call_target="tpu_custom_call" | custom-call | flops 500000000 | bytes 1048576 | tf_op jit(solution)/shard_map/pallas_call | solution.py:44
  2.8 0.0 copy-start.1
  2.8 0.0 copy-start.2
  2.9 48.3 %all_to_all.15.own_ref = bf16[32,160,128]{2,1,0:T(8,128)(2,1)S(1)} all-to-all(bf16[32,160,128]{2,1,0:T(8,128)(2,1)S(1)} %shard_map.185), channel_id=1, replica_groups=mesh['z'=8,'x'=4,'y'=8,'c'=2] {'z','x'}, dimensions={0} | all-to-all | bytes 2621440 | tf_op jit(solution)/shard_map/all_to_all | solution.py:251
  51.2 1.9 %collective-permute-start.7 = (bf16[32,160,128]{2,1,0:T(8,128)(2,1)S(1)}, bf16[32,160,128]{2,1,0:T(8,128)(2,1)S(1)}, u32[]{:S(2)}, u32[]{:S(2)}) collective-permute-start(bf16[32,160,128]{2,1,0:T(8,128)(2,1)S(1)} %all_to_all.15.own_ref), channel_id=1, source_target_pairs={{0,1},{1,0},{2,3},{3,2},{4,5},{5,4},{6,7},{7,6},{8,9},{9,8},{10,11... | collective-permute-start | bytes 3932168 | tf_op jit(solution)/shard_map/ppermute | solution.py:264
  53.1 0.0 copy-done.1
  53.1 0.0 copy-done.2
  53.1 0.0 copy-start
  53.1 1.7 %shard_map.186 = (f32[640,320]{1,0:T(8,128)S(1)}, f32[640,320]{1,0:T(8,128)S(1)}) custom-call(s32[1]{0:T(128)} %bitcast.6.core_ref, bf16[32,160,128]{2,1,0:T(8,128)(2,1)S(1)} %all_to_all.15.own_ref, bf16[320,2048]{1,0:T(8,128)(2,1)S(1)} %bitcast.19, bf16[320,2048]{1,0:T(8,128)(2,1)S(1)} %bitcast.21), custom_call_target="tpu_custom_call" | custom-call | flops 1000000000 | bytes 1048576 | tf_op jit(solution)/shard_map/pallas_call | solution.py:44
  54.9 1.2 collective-permute-done.7.other_ref
  56.1 0.0 copy-done
  56.1 2.6 %shard_map.187 = (bf16[640,320]{1,0:T(8,128)(2,1)S(1)}, bf16[8,640,128]{2,1,0:T(8,128)(2,1)S(1)}) custom-call(s32[1]{0:T(128)} %bitcast.6.core_ref, bf16[32,160,128]{2,1,0:T(8,128)(2,1)S(1)} %collective-permute-done.7.other_ref, bf16[320,2048]{1,0:T(8,128)(2,1)S(1)} %bitcast.20, bf16[320,2048]{1,0:T(8,128)(2,1)S(1)} %bitcast.22, ...), custom_call_target="tpu_custom_call" | custom-call | flops 2000000000 | bytes 1048576 | tf_op jit(solution)/shard_map/pallas_call | solution.py:44
  58.7 2.0 %collective-permute-start.8 = (bf16[8,640,128]{2,1,0:T(8,128)(2,1)S(1)}, bf16[8,640,128]{2,1,0:T(8,128)(2,1)S(1)}, u32[]{:S(2)}, u32[]{:S(2)}) collective-permute-start(bf16[8,640,128]{2,1,0:T(8,128)(2,1)S(1)} %get-tuple-element.21), channel_id=1, source_target_pairs={{0,1},{1,0},{2,3},{3,2},{4,5},{5,4},{6,7},{7,6},{8,9},{9,8},{10,11... | collective-permute-start | bytes 3932168 | tf_op jit(solution)/shard_map/ppermute | solution.py:264
  60.7 0.9 shard_map.188
  61.6 2.0 %collective-permute-done.8 = bf16[8,640,128]{2,1,0:T(8,128)(2,1)S(1)} collective-permute-done((bf16[8,640,128]{2,1,0:T(8,128)(2,1)S(1)}, bf16[8,640,128]{2,1,0:T(8,128)(2,1)S(1)}, u32[]{:S(2)}, u32[]{:S(2)}) %collective-permute-start.8) | collective-permute-done | bytes 1310752 | tf_op jit(solution)/shard_map/ppermute | solution.py:264
  63.6 1.4 %add_convert_fusion = bf16[8,640,128]{2,1,0:T(8,128)(2,1)} fusion(bf16[8,640,128]{2,1,0:T(8,128)(2,1)S(1)} %collective-permute-done.8, bf16[8,640,128]{2,1,0:T(8,128)(2,1)S(1)} %shard_map.188), kind=kLoop, calls=%fused_computation | loop fusion | flops 2621440 | bytes 3932160 | tf_op jit(solution)/shard_map/convert_element_type | solution.py:311
  65.1 0.0 copy-start.7
  65.1 0.0 copy-start.8
  65.1 0.0 copy-start.9
  65.1 0.0 copy-start.10
  65.1 7.7 %all-to-all-start.1 = ((bf16[8,640,128]{2,1,0:T(8,128)(2,1)}), bf16[8,640,128]{2,1,0:T(8,128)(2,1)S(1)}, u32[]{:S(2)}, u32[]{:S(2)}) async-start(bf16[8,640,128]{2,1,0:T(8,128)(2,1)} %add_convert_fusion), calls=%async_computation.1 | async-start | bytes 2621440 | tf_op jit(solution)/shard_map/all_to_all | solution.py:251
  72.8 0.0 copy-done.3
  72.8 0.0 copy-done.4
  72.8 0.0 copy-done.5
  72.8 0.2 shard_map.176
  73.0 2.1 %collective-permute-start = (bf16[8,512]{1,0:T(8,128)(2,1)S(1)}, bf16[8,512]{1,0:T(8,128)(2,1)S(1)}, u32[]{:S(2)}, u32[]{:S(2)}) collective-permute-start(bf16[8,512]{1,0:T(8,128)(2,1)S(1)} %shard_map.176), channel_id=1, source_target_pairs={{0,16},{16,32},{32,48},{48,64},{64,80},{80,96},{96,112},{112,128},... | collective-permute-start | bytes 24584 | tf_op jit(solution)/shard_map/ppermute | solution.py:256
  75.1 0.0 copy-done.14
  75.1 0.1 copy.22.rate_ref
  75.2 1.2 collective-permute-done.rim_ref
  76.5 0.0 copy-done.7
  76.5 0.0 copy-done.8
  76.5 0.0 copy-done.9
  76.5 0.0 copy-done.10
  76.5 0.0 copy-start.11
  76.5 0.0 copy-start.13
  76.5 0.0 copy-start.12
  76.5 2.2 %shard_map.177 = (bf16[256,384]{1,0:T(8,128)(2,1)S(1)}, bf16[128,384]{1,0:T(8,128)(2,1)S(1)}, bf16[128,384]{1,0:T(8,128)(2,1)S(1)}, f32[4,384]{1,0:T(4,128)S(1)}...) custom-call(s32[1]{0:T(128)} %bitcast.group_ref, bf16[256,384]{1,0:T(8,128)(2,1)S(1)} %copy-done.3, ...), custom_call_target="tpu_custom_call" | custom-call | flops 2000000000 | bytes 1048576 | tf_op jit(solution)/shard_map/pallas_call | solution.py:44
  78.8 4.2 %collective-permute-start.1 = (bf16[272,128]{1,0:T(8,128)(2,1)S(1)}, bf16[272,128]{1,0:T(8,128)(2,1)S(1)}, u32[]{:S(2)}, u32[]{:S(2)}) collective-permute-start(bf16[272,128]{1,0:T(8,128)(2,1)S(1)} %get-tuple-element.17), channel_id=1, source_target_pairs={{0,16},{16,32},{32,48},{48,64},{64,80},{80,96},{96,112},{112,128},... | collective-permute-start | bytes 208904 | tf_op jit(solution)/shard_map/ppermute | solution.py:256
  83.0 4.7 %collective-permute-start.2 = (bf16[272,128]{1,0:T(8,128)(2,1)S(1)}, bf16[272,128]{1,0:T(8,128)(2,1)S(1)}, u32[]{:S(2)}, u32[]{:S(2)}) collective-permute-start(bf16[272,128]{1,0:T(8,128)(2,1)S(1)} %get-tuple-element.17), channel_id=1, source_target_pairs={{0,32},{16,48},{32,64},{48,80},{64,96},{80,112},{96,128},{112,144}... | collective-permute-start | bytes 208904 | tf_op jit(solution)/shard_map/ppermute | solution.py:256
  87.6 0.0 collective-permute-done.1.after_ref
  87.6 1.9 %collective-permute-done.2.before_ref = bf16[272,128]{1,0:T(8,128)(2,1)S(1)} collective-permute-done((bf16[272,128]{1,0:T(8,128)(2,1)S(1)}, bf16[272,128]{1,0:T(8,128)(2,1)S(1)}, u32[]{:S(2)}, u32[]{:S(2)}) %collective-permute-start.2) | collective-permute-done | bytes 69664 | tf_op jit(solution)/shard_map/ppermute | solution.py:256
  89.6 5.8 %collective-permute-start.3 = (bf16[272,128]{1,0:T(8,128)(2,1)S(1)}, bf16[272,128]{1,0:T(8,128)(2,1)S(1)}, u32[]{:S(2)}, u32[]{:S(2)}) collective-permute-start(bf16[272,128]{1,0:T(8,128)(2,1)S(1)} %shard_map.179.after_ref), channel_id=1, source_target_pairs={{0,32},{16,48},{32,64},{48,80},{64,96},{80,112},{96,128},{112,144}... | collective-permute-start | bytes 208904 | tf_op jit(solution)/shard_map/ppermute | solution.py:256
  95.4 1.9 %collective-permute-done.3.before_ref = bf16[272,128]{1,0:T(8,128)(2,1)S(1)} collective-permute-done((bf16[272,128]{1,0:T(8,128)(2,1)S(1)}, bf16[272,128]{1,0:T(8,128)(2,1)S(1)}, u32[]{:S(2)}, u32[]{:S(2)}) %collective-permute-start.3) | collective-permute-done | bytes 69664 | tf_op jit(solution)/shard_map/ppermute | solution.py:256
  97.3 7.9 %collective-permute-start.4 = (bf16[272,128]{1,0:T(8,128)(2,1)S(1)}, bf16[272,128]{1,0:T(8,128)(2,1)S(1)}, u32[]{:S(2)}, u32[]{:S(2)}) collective-permute-start(bf16[272,128]{1,0:T(8,128)(2,1)S(1)} %shard_map.180.after_ref), channel_id=1, source_target_pairs={{0,64},{16,80},{32,96},{48,112},{64,128},{80,144},{96,160},{112,17... | collective-permute-start | bytes 208904 | tf_op jit(solution)/shard_map/ppermute | solution.py:256
  105.2 0.0 copy-done.11
  105.2 0.1 copy.24.routes_ref
  105.3 0.1 copy.23.gain_ref
  105.5 0.0 copy-done.12
  105.5 0.1 copy.25.logit_ref
  105.6 1.5 %collective-permute-done.4.before_ref = bf16[272,128]{1,0:T(8,128)(2,1)S(1)} collective-permute-done((bf16[272,128]{1,0:T(8,128)(2,1)S(1)}, bf16[272,128]{1,0:T(8,128)(2,1)S(1)}, u32[]{:S(2)}, u32[]{:S(2)}) %collective-permute-start.4) | collective-permute-done | bytes 69664 | tf_op jit(solution)/shard_map/ppermute | solution.py:256
  107.1 4.4 %collective-permute-start.5 = (bf16[272,128]{1,0:T(8,128)(2,1)S(1)}, bf16[272,128]{1,0:T(8,128)(2,1)S(1)}, u32[]{:S(2)}, u32[]{:S(2)}) collective-permute-start(bf16[272,128]{1,0:T(8,128)(2,1)S(1)} %shard_map.181.after_ref), channel_id=1, source_target_pairs={{0,128},{16,144},{32,160},{48,176},{64,192},{80,208},{96,224},{112... | collective-permute-start | bytes 208904 | tf_op jit(solution)/shard_map/ppermute | solution.py:256
  111.6 0.6 shard_map.190.weight_ref
  112.2 1.3 collective-permute-done.5.before_ref
  113.5 12.3 %collective-permute-start.6 = (bf16[272,128]{1,0:T(8,128)(2,1)S(1)}, bf16[272,128]{1,0:T(8,128)(2,1)S(1)}, u32[]{:S(2)}, u32[]{:S(2)}) collective-permute-start(bf16[272,128]{1,0:T(8,128)(2,1)S(1)} %shard_map.182.after_ref), channel_id=1, source_target_pairs={{0,256},{16,272},{32,288},{48,304},{64,320},{80,336},{96,352},{112... | collective-permute-start | bytes 208904 | tf_op jit(solution)/shard_map/ppermute | solution.py:256
  125.8 0.0 all-to-all-done.1.parts_ref
  125.8 1.0 shard_map.189
  126.8 3.9 %all-to-all-start.2 = ((bf16[32,24,128]{2,1,0:T(8,128)(2,1)}), bf16[32,24,128]{2,1,0:T(8,128)(2,1)S(1)}, u32[]{:S(2)}, u32[]{:S(2)}) async-start(bf16[32,24,128]{2,1,0:T(8,128)(2,1)} %shard_map.189), calls=%async_computation.2 | async-start | bytes 393216 | tf_op jit(solution)/shard_map/all_to_all | solution.py:251
  130.7 0.0 copy-start.6
  130.7 0.8 shard_map.178.y_ref
  131.6 0.0 collective-permute-done.6.before_ref
  131.6 0.0 copy-done.6
  131.6 1.0 shard_map.184
  132.6 9.2 %all-to-all-done.2.back_ref = bf16[32,24,128]{2,1,0:T(8,128)(2,1)S(1)} async-done(((bf16[32,24,128]{2,1,0:T(8,128)(2,1)}), bf16[32,24,128]{2,1,0:T(8,128)(2,1)S(1)}, u32[]{:S(2)}, u32[]{:S(2)}) %all-to-all-start.2) | async-done | bytes 196640 | tf_op jit(solution)/shard_map/all_to_all | solution.py:251
  141.8 0.9 shard_map.191
  (10 shorter events, 0.2 us)
Async XLA Ops:
  2.8 50.3 %copy-start.1 = (bf16[1,2048,320]{1,2,0:T(8,128)(2,1)S(1)}, bf16[1,2048,320]{1,2,0:T(8,128)(2,1)}, u32[]{:S(2)}) copy-start(bf16[1,2048,320]{1,2,0:T(8,128)(2,1)} %param.31) | copy-start | bytes 3932164
  2.8 50.3 %copy-start.2 = (bf16[1,2048,320]{1,2,0:T(8,128)(2,1)S(1)}, bf16[1,2048,320]{1,2,0:T(8,128)(2,1)}, u32[]{:S(2)}) copy-start(bf16[1,2048,320]{1,2,0:T(8,128)(2,1)} %param.32) | copy-start | bytes 3932164
  51.2 4.9 %collective-permute-start.7 = (bf16[32,160,128]{2,1,0:T(8,128)(2,1)S(1)}, bf16[32,160,128]{2,1,0:T(8,128)(2,1)S(1)}, u32[]{:S(2)}, u32[]{:S(2)}) collective-permute-start(bf16[32,160,128]{2,1,0:T(8,128)(2,1)S(1)} %all_to_all.15.own_ref), channel_id=1, source_target_pairs={{0,1},{1,0},{2,3},{3,2},{4,5},{5,4},{6,7},{7,6},{8,9},{9,8},{10,11... | collective-permute-start | bytes 3932168 | tf_op jit(solution)/shard_map/ppermute | solution.py:264
  53.1 3.0 %copy-start = (bf16[1,320,2048]{2,1,0:T(8,128)(2,1)S(1)}, bf16[1,320,2048]{2,1,0:T(8,128)(2,1)}, u32[]{:S(2)}) copy-start(bf16[1,320,2048]{2,1,0:T(8,128)(2,1)} %param.33) | copy-start | bytes 3932164
  58.7 4.9 %collective-permute-start.8 = (bf16[8,640,128]{2,1,0:T(8,128)(2,1)S(1)}, bf16[8,640,128]{2,1,0:T(8,128)(2,1)S(1)}, u32[]{:S(2)}, u32[]{:S(2)}) collective-permute-start(bf16[8,640,128]{2,1,0:T(8,128)(2,1)S(1)} %get-tuple-element.21), channel_id=1, source_target_pairs={{0,1},{1,0},{2,3},{3,2},{4,5},{5,4},{6,7},{7,6},{8,9},{9,8},{10,11... | collective-permute-start | bytes 3932168 | tf_op jit(solution)/shard_map/ppermute | solution.py:264
  65.0 7.8 %copy-start.3 = (bf16[256,384]{1,0:T(8,128)(2,1)S(1)}, bf16[256,384]{1,0:T(8,128)(2,1)}, u32[]{:S(2)}) copy-start(bf16[256,384]{1,0:T(8,128)(2,1)} %x_hbm.3) | copy-start | bytes 589828
  65.0 7.8 %copy-start.4 = (bf16[256,384]{1,0:T(8,128)(2,1)S(1)}, bf16[256,384]{1,0:T(8,128)(2,1)}, u32[]{:S(2)}) copy-start(bf16[256,384]{1,0:T(8,128)(2,1)} %b_hbm.3) | copy-start | bytes 589828
  65.0 7.8 %copy-start.5 = (bf16[256,384]{1,0:T(8,128)(2,1)S(1)}, bf16[256,384]{1,0:T(8,128)(2,1)}, u32[]{:S(2)}) copy-start(bf16[256,384]{1,0:T(8,128)(2,1)} %c_hbm.3) | copy-start | bytes 589828
  65.0 10.1 %copy-start.14 = (f32[4]{0:T(128)S(1)}, f32[4]{0:T(128)}, u32[]{:S(2)}) copy-start(f32[4]{0:T(128)} %param.20) | copy-start | bytes 52
  65.1 11.4 %copy-start.7 = (f32[4,384]{1,0:T(4,128)S(1)}, f32[4,384]{1,0:T(4,128)}, u32[]{:S(2)}) copy-start(f32[4,384]{1,0:T(4,128)} %dt_ref.1) | copy-start | bytes 18436
  65.1 11.4 %copy-start.8 = (f32[256,4]{0,1:T(4,128)S(1)}, f32[256,4]{0,1:T(4,128)}, u32[]{:S(2)}) copy-start(f32[256,4]{0,1:T(4,128)} %param.23) | copy-start | bytes 12292
  65.1 11.4 %copy-start.9 = (f32[256,4]{0,1:T(4,128)S(1)}, f32[256,4]{0,1:T(4,128)}, u32[]{:S(2)}) copy-start(f32[256,4]{0,1:T(4,128)} %param.24) | copy-start | bytes 12292
  65.1 11.4 %copy-start.10 = (f32[256,4]{0,1:T(4,128)S(1)}, f32[256,4]{0,1:T(4,128)}, u32[]{:S(2)}) copy-start(f32[256,4]{0,1:T(4,128)} %param.25) | copy-start | bytes 12292
  65.1 60.7 %all-to-all-start.1 = ((bf16[8,640,128]{2,1,0:T(8,128)(2,1)}), bf16[8,640,128]{2,1,0:T(8,128)(2,1)S(1)}, u32[]{:S(2)}, u32[]{:S(2)}) async-start(bf16[8,640,128]{2,1,0:T(8,128)(2,1)} %add_convert_fusion), calls=%async_computation.1 | async-start | bytes 2621440 | tf_op jit(solution)/shard_map/all_to_all | solution.py:251
  73.0 3.5 %collective-permute-start = (bf16[8,512]{1,0:T(8,128)(2,1)S(1)}, bf16[8,512]{1,0:T(8,128)(2,1)S(1)}, u32[]{:S(2)}, u32[]{:S(2)}) collective-permute-start(bf16[8,512]{1,0:T(8,128)(2,1)S(1)} %shard_map.176), channel_id=1, source_target_pairs={{0,16},{16,32},{32,48},{48,64},{64,80},{80,96},{96,112},{112,128},... | collective-permute-start | bytes 24584 | tf_op jit(solution)/shard_map/ppermute | solution.py:256
  76.5 28.7 %copy-start.11 = (s32[160,2]{0,1:T(2,128)S(1)}, s32[160,2]{0,1:T(2,128)}, u32[]{:S(2)}) copy-start(s32[160,2]{0,1:T(2,128)} %param.29) | copy-start | bytes 3844
  76.5 28.8 %copy-start.13 = (f32[256]{0:T(256)S(1)}, f32[256]{0:T(256)}, u32[]{:S(2)}) copy-start(f32[256]{0:T(256)} %param.26) | copy-start | bytes 3076
  76.5 28.9 %copy-start.12 = (f32[160,2]{0,1:T(2,128)S(1)}, f32[160,2]{0,1:T(2,128)}, u32[]{:S(2)}) copy-start(f32[160,2]{0,1:T(2,128)} %param.30) | copy-start | bytes 3844
  78.8 8.9 %collective-permute-start.1 = (bf16[272,128]{1,0:T(8,128)(2,1)S(1)}, bf16[272,128]{1,0:T(8,128)(2,1)S(1)}, u32[]{:S(2)}, u32[]{:S(2)}) collective-permute-start(bf16[272,128]{1,0:T(8,128)(2,1)S(1)} %get-tuple-element.17), channel_id=1, source_target_pairs={{0,16},{16,32},{32,48},{48,64},{64,80},{80,96},{96,112},{112,128},... | collective-permute-start | bytes 208904 | tf_op jit(solution)/shard_map/ppermute | solution.py:256
  83.0 6.6 %collective-permute-start.2 = (bf16[272,128]{1,0:T(8,128)(2,1)S(1)}, bf16[272,128]{1,0:T(8,128)(2,1)S(1)}, u32[]{:S(2)}, u32[]{:S(2)}) collective-permute-start(bf16[272,128]{1,0:T(8,128)(2,1)S(1)} %get-tuple-element.17), channel_id=1, source_target_pairs={{0,32},{16,48},{32,64},{48,80},{64,96},{80,112},{96,128},{112,144}... | collective-permute-start | bytes 208904 | tf_op jit(solution)/shard_map/ppermute | solution.py:256
  89.6 7.7 %collective-permute-start.3 = (bf16[272,128]{1,0:T(8,128)(2,1)S(1)}, bf16[272,128]{1,0:T(8,128)(2,1)S(1)}, u32[]{:S(2)}, u32[]{:S(2)}) collective-permute-start(bf16[272,128]{1,0:T(8,128)(2,1)S(1)} %shard_map.179.after_ref), channel_id=1, source_target_pairs={{0,32},{16,48},{32,64},{48,80},{64,96},{80,112},{96,128},{112,144}... | collective-permute-start | bytes 208904 | tf_op jit(solution)/shard_map/ppermute | solution.py:256
  97.3 9.8 %collective-permute-start.4 = (bf16[272,128]{1,0:T(8,128)(2,1)S(1)}, bf16[272,128]{1,0:T(8,128)(2,1)S(1)}, u32[]{:S(2)}, u32[]{:S(2)}) collective-permute-start(bf16[272,128]{1,0:T(8,128)(2,1)S(1)} %shard_map.180.after_ref), channel_id=1, source_target_pairs={{0,64},{16,80},{32,96},{48,112},{64,128},{80,144},{96,160},{112,17... | collective-permute-start | bytes 208904 | tf_op jit(solution)/shard_map/ppermute | solution.py:256
  107.1 6.3 %collective-permute-start.5 = (bf16[272,128]{1,0:T(8,128)(2,1)S(1)}, bf16[272,128]{1,0:T(8,128)(2,1)S(1)}, u32[]{:S(2)}, u32[]{:S(2)}) collective-permute-start(bf16[272,128]{1,0:T(8,128)(2,1)S(1)} %shard_map.181.after_ref), channel_id=1, source_target_pairs={{0,128},{16,144},{32,160},{48,176},{64,192},{80,208},{96,224},{112... | collective-permute-start | bytes 208904 | tf_op jit(solution)/shard_map/ppermute | solution.py:256
  113.5 18.0 %collective-permute-start.6 = (bf16[272,128]{1,0:T(8,128)(2,1)S(1)}, bf16[272,128]{1,0:T(8,128)(2,1)S(1)}, u32[]{:S(2)}, u32[]{:S(2)}) collective-permute-start(bf16[272,128]{1,0:T(8,128)(2,1)S(1)} %shard_map.182.after_ref), channel_id=1, source_target_pairs={{0,256},{16,272},{32,288},{48,304},{64,320},{80,336},{96,352},{112... | collective-permute-start | bytes 208904 | tf_op jit(solution)/shard_map/ppermute | solution.py:256
  126.8 15.0 %all-to-all-start.2 = ((bf16[32,24,128]{2,1,0:T(8,128)(2,1)}), bf16[32,24,128]{2,1,0:T(8,128)(2,1)S(1)}, u32[]{:S(2)}, u32[]{:S(2)}) async-start(bf16[32,24,128]{2,1,0:T(8,128)(2,1)} %shard_map.189), calls=%async_computation.2 | async-start | bytes 393216 | tf_op jit(solution)/shard_map/all_to_all | solution.py:251
  130.7 0.9 copy-start.6

commit v3 on v1

--- a/solution.py
+++ b/solution.py
@@ -99,10 +99,7 @@
     return jnp.concatenate(parts, axis=1)
 
 
-def prep_kernel(
-    core_ref, rows_hbm, gain_hbm, routes_hbm, out_ref, rows_ref, gain_ref, routes_ref, sems
-):
-    fetch(((rows_hbm, rows_ref), (gain_hbm, gain_ref), (routes_hbm, routes_ref)), sems)
+def prep_kernel(core_ref, rows_ref, gain_ref, routes_ref, out_ref):
     tokens, features = rows_ref.shape
     half = features // 2
     low = pl.multiple_of(core_ref[0] * half, half)
@@ -164,11 +161,6 @@
     up_out[...] = over_last(rows, up_ref[:, pl.ds(low, half)])
 
 
-def store_blocks(ref, value):
-    for j in range(N_BLK):
-        ref[j] = value[:, LANES * j : LANES * (j + 1)].astype(BF16)
-
-
 def down_columns(down_ref, parity):
     parts = []
     for j in range(N_BLK):
@@ -178,7 +170,7 @@
 
 
 def second_half_kernel(
-    core_ref, other_ref, gate_ref, up_ref, down_ref, gate_in, up_in, hidden_out, out_ref
+    core_ref, other_ref, gate_ref, up_ref, gate_in, up_in, hidden_out
 ):
     half = gate_ref.shape[1] // 2
     other = 1 - core_ref[0]
@@ -188,11 +180,21 @@
     up = up_in[...] + over_last(rows, up_ref[:, pl.ds(low, half)])
     hidden = (gate * jax.nn.sigmoid(gate) * up).astype(BF16)
     hidden_out[...] = hidden
-    store_blocks(out_ref, dot(hidden, down_columns(down_ref, other)))
-
-
-def own_down_kernel(core_ref, hidden_ref, down_ref, out_ref):
-    store_blocks(out_ref, dot(hidden_ref[...], down_columns(down_ref, core_ref[0])))
+
+
+def pick_kernel(core_ref, down_ref, own_out, other_out):
+    own_out[...] = down_columns(down_ref, core_ref[0])
+    other_out[...] = down_columns(down_ref, 1 - core_ref[0])
+
+
+def own_down_kernel(hidden_ref, down_ref, out_ref):
+    out_ref[...] = dot(hidden_ref[...], down_ref[...])
+
+
+def other_down_kernel(hidden_ref, down_ref, own_ref, out_ref):
+    value = own_ref[...] + dot(hidden_ref[...], down_ref[...])
+    for j in range(N_BLK):
+        out_ref[j] = value[:, LANES * j : LANES * (j + 1)].astype(BF16)
 
 
 def collect_kernel(parts_ref, out_ref):
@@ -256,6 +258,11 @@
     return lax.ppermute(value, EP, [(k, k + steps) for k in range(count - steps)])
 
 
+def rows_behind(value, steps):
+    count = lax.axis_size("z")
+    return lax.ppermute(value, "z", [(k, k + steps) for k in range(count - steps)])
+
+
 def join(after, before):
     return call(join_kernel, sds(after.shape, BF16), (after, before), 10**8, vmem=4)
 
@@ -264,61 +271,94 @@
     return lax.ppermute(value, "c", [(0, 1), (1, 0)])
 
 
-def dispatch(moe_rows, moe_gain, routes):
-    core = lax.axis_index("c").astype(jnp.int32)[None]
-    outbox = call(
-        prep_kernel,
-        sds((N_EXP, CHUNK, LANES), BF16),
-        (core, moe_rows, moe_gain[None, :], routes.T),
-        5 * 10**8,
+def in_hbm(*arrays):
+    return tuple(pltpu.with_memory_space_constraint(a, pltpu.HBM) for a in arrays)
+
+
+def first_loads(group, x_in, b_in, c_in, moe_rows, moe_gain, routes):
+    rows = x_in.shape[0] + 2 * NSTATE
+    given = in_hbm(x_in, b_in, c_in, moe_rows, moe_gain[None, :], routes.T)
+    return call(
+        rim_kernel,
+        (sds((8, rows), BF16), *(sds(a.shape, a.dtype) for a in given[3:])),
+        (group, *given),
+        10**8,
         smem=1,
-        hbm=3,
+        hbm=6,
+        vmem=4,
         scratch=(
-            pltpu.VMEM(moe_rows.shape, BF16),
-            pltpu.VMEM((1, moe_gain.shape[0]), F32),
-            pltpu.VMEM(routes.shape[::-1], jnp.int32),
-            pltpu.SemaphoreType.DMA((3,)),
+            pltpu.VMEM((x_in.shape[0], LANES), BF16),
+            pltpu.VMEM((NSTATE, LANES), BF16),
+            pltpu.VMEM((NSTATE, LANES), BF16),
+            pltpu.SemaphoreType.DMA((6,)),
         ),
     )
-    return core, outbox
-
-
-def run_experts(core, own, w_gate, w_up, w_down):
+
+
+def down_halves(core, down):
+    half = sds((down.shape[0], down.shape[1] // 2), BF16)
+    own, theirs = call(pick_kernel, (half, half), (core, down), 10**8, smem=1)
+    return own, swap_cores(theirs)
+
+
+def run_experts(core, own, w_gate, w_up, down_own, down_other):
     rows, hidden_units = (N_EXP * CAP, w_gate.shape[2])
-    gate, up, down = (w_gate[0].T, w_up[0].T, w_down[0])
+    gate, up = (w_gate[0].T, w_up[0].T)
     other = swap_cores(own)
     half_act = sds((rows, hidden_units), F32)
     gate_act, up_act = call(
         first_half_kernel, (half_act, half_act), (core, own, gate, up), 10**9, smem=1, vmem=20
     )
-    packed = sds((N_BLK, rows, LANES), BF16)
-    hidden, theirs = call(
+    hidden = call(
         second_half_kernel,
-        (sds((rows, hidden_units), BF16), packed),
-        (core, other, gate, up, down, gate_act, up_act),
+        sds((rows, hidden_units), BF16),
+        (core, other, gate, up, gate_act, up_act),
         2 * 10**9,
         smem=1,
-        vmem=24,
-    )
-    arrived = swap_cores(theirs)
-    mine = call(own_down_kernel, packed, (core, hidden, down), 6 * 10**8, smem=1, vmem=16)
-    return (mine.astype(F32) + arrived.astype(F32)).astype(BF16)
-
-
-def rim_kernel(group_ref, x_hbm, b_hbm, c_hbm, out_ref, x_ref, b_ref, c_ref, sems):
-    low = pl.multiple_of(group_ref[0] * NSTATE, NSTATE)
-    length = x_hbm.shape[1]
-    last = pl.ds(length - LANES, LANES)
-    fetch(
-        (
-            (x_hbm.at[:, last], x_ref),
-            (b_hbm.at[pl.ds(low, NSTATE), last], b_ref),
-            (c_hbm.at[pl.ds(low, NSTATE), last], c_ref),
-        ),
-        sems,
-    )
+        vmem=20,
+    )
+    partner = swap_cores(hidden)
+    mine = call(
+        own_down_kernel,
+        sds((rows, down_own.shape[1]), F32),
+        (hidden, down_own),
+        6 * 10**8,
+        vmem=12,
+    )
+    return call(
+        other_down_kernel,
+        sds((N_BLK, rows, LANES), BF16),
+        (partner, down_other, mine),
+        6 * 10**8,
+        vmem=12,
+    )
+
+
+def rim_kernel(
+    group_ref, x_hbm, b_hbm, c_hbm, rows_hbm, gain_hbm, routes_hbm,
+    out_ref, rows_out, gain_out, routes_out, x_ref, b_ref, c_ref, sems,
+):
+    group = pl.ds(pl.multiple_of(group_ref[0] * NSTATE, NSTATE), NSTATE)
+    last = pl.ds(x_hbm.shape[1] - LANES, LANES)
+    pairs = (
+        (x_hbm.at[:, last], x_ref),
+        (b_hbm.at[group, last], b_ref),
+        (c_hbm.at[group, last], c_ref),
+        (rows_hbm, rows_out),
+        (gain_hbm, gain_out),
+        (routes_hbm, routes_out),
+    )
+    copies = [
+        pltpu.make_async_copy(source, target, sems.at[k]) for k, (source, target) in enumerate(pairs)
+    ]
+    for copy in copies:
+        copy.start()
+    for copy in copies[:3]:
+        copy.wait()
     rows = jnp.concatenate([r[...].astype(F32) for r in (x_ref, b_ref, c_ref)], axis=0)
     out_ref[...] = rows.T[LANES - 8 :, :].astype(BF16)
+    for copy in copies[3:]:
+        copy.wait()
 
 
 def conv(signal, rim, taps):
@@ -414,27 +454,63 @@
             y_out[rows, here] = dot(x_ref[rows, :size], mask.astype(BF16))
 
 
+def state_and_decays(ref):
+    size = ref.shape[0] - 16
+    value = ref[...].astype(F32)
+    pairs = range(size, size + 2 * (size // HEAD_DIM), 2)
+    return value[:size], [value[k : k + 1] + value[k + 1 : k + 2] for k in pairs]
+
+
+def joined(after, before):
+    states = [
+        after[0][HEAD_DIM * h : HEAD_DIM * (h + 1)] + d * before[0][HEAD_DIM * h : HEAD_DIM * (h + 1)]
+        for h, d in enumerate(after[1])
+    ]
+    return jnp.concatenate(states, axis=0), [a * b for a, b in zip(after[1], before[1])]
+
+
+def store_spans(ref, value):
+    size = ref.shape[0] - 16
+    ref[:size, :] = value[0].astype(BF16)
+    rows = []
+    for total in value[1]:
+        high = total.astype(BF16).astype(F32)
+        rows += [high, total - high]
+    ref[size:, :] = in_rows(rows).astype(BF16)
+
+
 def join_kernel(after_ref, before_ref, out_ref):
-    size = after_ref.shape[0] - 16
-    after = after_ref[...].astype(F32)
-    before = before_ref[...].astype(F32)
-    decays = []
-    for h in range(size // HEAD_DIM):
-        rows = slice(HEAD_DIM * h, HEAD_DIM * (h + 1))
-        pair = slice(size + 2 * h, size + 2 * h + 1)
-        rest = slice(size + 2 * h + 1, size + 2 * h + 2)
-        own = after[pair] + after[rest]
-        out_ref[rows, :] = (after[rows] + own * before[rows]).astype(BF16)
-        total = own * (before[pair] + before[rest])
-        high = total.astype(BF16).astype(F32)
-        decays += [high, total - high]
-    out_ref[size:, :] = in_rows(decays).astype(BF16)
-
-
-def mixed_kernel(y_ref, before_ref, c_ref, cum_ref, z_ref, gain_ref, out_ref):
+    store_spans(out_ref, joined(state_and_decays(after_ref), state_and_decays(before_ref)))
+
+
+def row_kernel(place_ref, own_ref, first_ref, second_ref, third_ref, before_out, total_out):
+    place = place_ref[0]
+    sources = [state_and_decays(r) for r in (own_ref, first_ref, second_ref, third_ref)]
+    heads = len(sources[0][1])
+    running = (jnp.zeros(sources[0][0].shape, F32), [jnp.ones((1, LANES), F32)] * heads)
+    before = running
+    for j in range(4):
+        back = (place - j) & 3
+        state, decays = sources[0]
+        for k in range(1, 4):
+            here = back == k
+            state = jnp.where(here, sources[k][0], state)
+            decays = [jnp.where(here, a, b) for a, b in zip(sources[k][1], decays)]
+        running = joined((state, decays), running)
+        ahead = j < place
+        before = (
+            jnp.where(ahead, running[0], before[0]),
+            [jnp.where(ahead, a, b) for a, b in zip(running[1], before[1])],
+        )
+    store_spans(before_out, before)
+    store_spans(total_out, running)
+
+
+def mixed_kernel(y_ref, row_ref, far_ref, c_ref, cum_ref, z_ref, gain_ref, out_ref):
     heads = cum_ref.shape[0]
     reach = jnp.exp(cum_ref[...])
-    carried = dot(before_ref[: heads * HEAD_DIM, :], c_ref[...])
+    before = joined(state_and_decays(row_ref), state_and_decays(far_ref))[0]
+    carried = dot(before.astype(BF16), c_ref[...])
     for h in range(heads):
         rows = slice(HEAD_DIM * h, HEAD_DIM * (h + 1))
         z = z_ref[rows, :].astype(F32)
@@ -442,26 +518,6 @@
         gated = y * (z * jax.nn.sigmoid(z))
         scale = lax.rsqrt(jnp.mean(gated * gated, axis=0, keepdims=True) + HEAD_EPS)
         out_ref[rows, :] = (gated * scale * gain_ref[rows, :]).astype(BF16)
-
-
-def rims_of(group, x_in, b_in, c_in):
-    rows = x_in.shape[0] + 2 * NSTATE
-    own = call(
-        rim_kernel,
-        sds((8, rows), BF16),
-        (group, x_in, b_in, c_in),
-        10**8,
-        smem=1,
-        hbm=3,
-        vmem=4,
-        scratch=(
-            pltpu.VMEM((x_in.shape[0], LANES), BF16),
-            pltpu.VMEM((NSTATE, LANES), BF16),
-            pltpu.VMEM((NSTATE, LANES), BF16),
-            pltpu.SemaphoreType.DMA((3,)),
-        ),
-    )
-    return from_behind(own, 1)
 
 
 def on_device(
@@ -485,11 +541,14 @@
 ):
     heads, length = dt_raw.shape
     values = x_in.shape[0]
-    core, outbox = dispatch(moe_rows, moe_gain, routes)
+    core = lax.axis_index("c").astype(jnp.int32)[None]
     group = lax.axis_index(TP) * heads // (HEADS // GROUPS)
     group = group.astype(jnp.int32)[None]
-    rims = rims_of(group, x_in, b_in, c_in)
+    own_rim, *tokens = first_loads(group, x_in, b_in, c_in, moe_rows, moe_gain, routes)
+    rims = from_behind(own_rim, 1)
+    outbox = call(prep_kernel, sds((N_EXP, CHUNK, LANES), BF16), (core, *tokens), 5 * 10**8, smem=1)
     arrived = exchange(outbox, EP)
+    down_parts = down_halves(core, w_down[0])
     x_conv, b_conv, c_conv, cum, step_dt, sent = call(
         local_kernel,
         (
@@ -514,17 +573,27 @@
             pltpu.SemaphoreType.DMA((3,)),
         ),
     )
-    nearest = from_behind(sent, 1)
-    second = from_behind(sent, 2)
+    in_order = [
+        lax.ppermute(sent, "x", [(k, (k + step) % 4) for k in range(4)]) for step in (1, 2, 3)
+    ]
     y_local = call(
         inner_kernel,
         sds((values, length), F32),
         (x_conv, b_conv, c_conv, cum, step_dt),
-        2 * 10**9,
-    )
+        2 * 10**8,
+    )
+    in_row, spans = call(
+        row_kernel,
+        (sds(sent.shape, BF16), sds(sent.shape, BF16)),
+        (lax.axis_index("x").astype(jnp.int32)[None], sent, *in_order),
+        10**8,
+        smem=1,
+    )
+    nearest = rows_behind(spans, 1)
+    second = rows_behind(spans, 2)
     spans = join(nearest, second)
-    for steps in (2, 4, 8, 16):
-        behind = from_behind(spans, steps)
+    for steps in (2, 4):
+        behind = rows_behind(spans, steps)
         spans = join(spans, behind)
     weights = call(
         weights_kernel,
@@ -532,7 +601,7 @@
         (routes, route_logit),
         10**9,
     )
-    partial = run_experts(core, arrived, w_gate, w_up, w_down)
+    partial = run_experts(core, arrived, w_gate, w_up, *down_parts)
     parts = exchange(partial, "y")
     collected = call(
         collect_kernel, sds((N_EXP, HEAD_ROWS + 8, LANES), BF16), (parts,), 10**8
@@ -541,7 +610,7 @@
     mixed = call(
         mixed_kernel,
         sds((values, length), BF16),
-        (y_local, spans, c_conv, cum, z_in, head_gain[:, None]),
+        (y_local, in_row, spans, c_conv, cum, z_in, head_gain[:, None]),
         2 * 10**9,
     )
     moe_out = call(

time: 145 us -> 130 us (0.90)
  waiting for transfers between devices: 20.4 us -> 7.73 us
  local copies, waits for them, and re-layouts: 3 us -> 0.52 us
  Pallas kernels: 13.3 us -> 15.7 us
    ppermute x7 -> x1, starting transfers between devices: 41.3 us -> 2.12 us  [from_behind(): lax.ppermute(value, EP, [(k, k + steps) for k in range(count - steps)])]
    ppermute x0 -> x7, starting transfers between devices: none -> 32.2 us  [the longest x4 20 us: rows_behind(): lax.ppermute(value, 'z', [(k, k + steps) for k in range(count - steps)])]
    all_to_all x2, waiting for transfers between devices: 9.22 us -> 0.22 us  [exchange(): return lax.all_to_all(value, axes, split_axis=0, concat_axis=0, tiled=True)]
    ppermute x7 -> x1, waiting for transfers between devices: 7.94 us -> 1.25 us  [from_behind(): lax.ppermute(value, EP, [(k, k + steps) for k in range(count - steps)])]
    ppermute x0 -> x7, waiting for transfers between devices: none -> 5.28 us  [the longest x3 2.87 us: on_device(): lax.ppermute(sent, 'x', [(k, (k + step) % 4) for k in range(4)])]
    all_to_all x2, starting transfers between devices: 11.6 us -> 15.2 us  [exchange(): return lax.all_to_all(value, axes, split_axis=0, concat_axis=0, tiled=True)]
    unnamed x38 -> x32, local copies, waits for them, and re-layouts: 2.77 us -> 0.29 us
    ppermute x2 -> x3, starting transfers between devices: 3.95 us -> 6.37 us  [swap_cores(): return lax.ppermute(value, 'c', [(0, 1), (1, 0)])]
  transfers between devices with their start and end apart: 11 -> 13, of which waited for: 8 -> 6; matrix products, arithmetic and copies ran while one was open for 0% -> 0% of each run, Pallas kernels for 6% -> 8%
where the time goes in v3:
time: 130 us; the launch traced here: 129 us
  starting transfers between devices  55.9 us (43%)
  blocking collectives  48.4 us (37%)
  Pallas kernels  15.7 us (12%)
  waiting for transfers between devices  7.73 us (6%)
    all_to_all x1, blocking collectives, exchange(): return lax.all_to_all(value, axes, split_axis=0, concat_axis=0, tiled=True)  48.4 us
    ppermute x4, starting transfers between devices, rows_behind(): lax.ppermute(value, 'z', [(k, k + steps) for k in range(count - steps)])  20 us
    pallas_call x17, Pallas kernels, call(): pl.pallas_call(kernel, out_shape=out_shape, in_specs=specs, out_specs=jax...  15.7 us
    all_to_all x2, starting transfers between devices, exchange(): return lax.all_to_all(value, axes, split_axis=0, concat_axis=0, tiled=True)  15.2 us
    ppermute x3, starting transfers between devices, on_device(): lax.ppermute(sent, 'x', [(k, (k + step) % 4) for k in range(4)])  12.2 us
    ppermute x3, starting transfers between devices, swap_cores(): return lax.ppermute(value, 'c', [(0, 1), (1, 0)])  6.37 us
    ppermute x3, waiting for transfers between devices, on_device(): lax.ppermute(sent, 'x', [(k, (k + step) % 4) for k in range(4)])  2.87 us
  transfers between devices with their start and end apart: 13, of which 6 were waited for; matrix products, arithmetic and copies ran while one was open for 0% of the time, Pallas kernels for 8%

profile of v3, /device:TPU:8, one launch (start us, length us, event | category | flops | bytes accessed | tf_op | source)
XLA Modules:
  0.0 129.2 jit_solution(11692754977070537121)
XLA Ops:
  0.6 1.2 shard_map.176
  1.9 1.1 shard_map.184
  3.0 0.0 copy-start
  3.0 0.0 copy-start.2
  3.0 48.4 %all_to_all.15.own_ref = bf16[32,160,128]{2,1,0:T(8,128)(2,1)S(1)} all-to-all(bf16[32,160,128]{2,1,0:T(8,128)(2,1)S(1)} %shard_map.184), channel_id=1, replica_groups=mesh['z'=8,'x'=4,'y'=8,'c'=2] {'z','x'}, dimensions={0} | all-to-all | bytes 2621440 | tf_op jit(solution)/shard_map/all_to_all | solution.py:253
  51.3 2.0 %collective-permute-start.8 = (bf16[32,160,128]{2,1,0:T(8,128)(2,1)S(1)}, bf16[32,160,128]{2,1,0:T(8,128)(2,1)S(1)}, u32[]{:S(2)}, u32[]{:S(2)}) collective-permute-start(bf16[32,160,128]{2,1,0:T(8,128)(2,1)S(1)} %all_to_all.15.own_ref), channel_id=1, source_target_pairs={{0,1},{1,0},{2,3},{3,2},{4,5},{5,4},{6,7},{7,6},{8,9},{9,8},{10,11... | collective-permute-start | bytes 3932168 | tf_op jit(solution)/shard_map/ppermute | solution.py:271
  53.4 0.0 copy-done
  53.4 0.3 shard_map.187
  53.7 2.4 %collective-permute-start.10 = (bf16[320,1024]{1,0:T(8,128)(2,1)S(1)}, bf16[320,1024]{1,0:T(8,128)(2,1)S(1)}, u32[]{:S(2)}, u32[]{:S(2)}) collective-permute-start(bf16[320,1024]{1,0:T(8,128)(2,1)S(1)} %get-tuple-element.32), channel_id=1, source_target_pairs={{0,1},{1,0},{2,3},{3,2},{4,5},{5,4},{6,7},{7,6},{8,9},{9,8},{10,11... | collective-permute-start | bytes 1966088 | tf_op jit(solution)/shard_map/ppermute | solution.py:271
  56.2 0.0 copy-done.2
  56.2 0.0 copy-done.1
  56.2 1.7 %shard_map.185 = (f32[640,320]{1,0:T(8,128)S(1)}, f32[640,320]{1,0:T(8,128)S(1)}) custom-call(s32[1]{0:T(128)} %bitcast.9.core_ref, bf16[32,160,128]{2,1,0:T(8,128)(2,1)S(1)} %all_to_all.15.own_ref, bf16[320,2048]{1,0:T(8,128)(2,1)S(1)} %bitcast.19, bf16[320,2048]{1,0:T(8,128)(2,1)S(1)} %bitcast.21), custom_call_target="tpu_custom_call" | custom-call | flops 1000000000 | bytes 1048576 | tf_op jit(solution)/shard_map/pallas_call | solution.py:44
  57.9 0.0 collective-permute-done.8.other_ref
  57.9 1.8 %shard_map.186.hidden_ref = bf16[640,320]{1,0:T(8,128)(2,1)S(1)} custom-call(s32[1]{0:T(128)} %bitcast.9.core_ref, bf16[32,160,128]{2,1,0:T(8,128)(2,1)S(1)} %collective-permute-done.8.other_ref, bf16[320,2048]{1,0:T(8,128)(2,1)S(1)} %bitcast.20, bf16[320,2048]{1,0:T(8,128)(2,1)S(1)} %bitcast.22, f32[640,320]{1,0:T(8,128)S(1)} %get-tuple-element.30.gate_in, ...), custom_call_target="tpu_custom_call" | custom-call | flops 2000000000 | bytes 1048576 | tf_op jit(solution)/shard_map/pallas_call | solution.py:44
  59.8 1.9 %collective-permute-start.9 = (bf16[640,320]{1,0:T(8,128)(2,1)S(1)}, bf16[640,320]{1,0:T(8,128)(2,1)S(1)}, u32[]{:S(2)}, u32[]{:S(2)}) collective-permute-start(bf16[640,320]{1,0:T(8,128)(2,1)S(1)} %shard_map.186.hidden_ref), channel_id=1, source_target_pairs={{0,1},{1,0},{2,3},{3,2},{4,5},{5,4},{6,7},{7,6},{8,9},{9,8},{10,11... | collective-permute-start | bytes 1228808 | tf_op jit(solution)/shard_map/ppermute | solution.py:271
  61.7 0.8 shard_map.188.own_ref
  62.6 0.0 collective-permute-done.10.down_ref
  62.6 1.0 collective-permute-done.9.hidden_ref
  63.5 1.9 %shard_map.189 = bf16[8,640,128]{2,1,0:T(8,128)(2,1)} custom-call(bf16[640,320]{1,0:T(8,128)(2,1)S(1)} %collective-permute-done.9.hidden_ref, bf16[320,1024]{1,0:T(8,128)(2,1)S(1)} %collective-permute-done.10.down_ref, f32[640,1024]{1,0:T(8,128)S(1)} %shard_map.188.own_ref), custom_call_target="tpu_custom_call" | custom-call | flops 600000000 | bytes 1048576 | tf_op jit(solution)/shard_map/pallas_call | solution.py:44
  65.5 0.0 copy-start.7
  65.5 0.0 copy-start.8
  65.5 0.0 copy-start.9
  65.5 0.0 copy-start.10
  65.5 7.7 %all-to-all-start.1 = ((bf16[8,640,128]{2,1,0:T(8,128)(2,1)}), bf16[8,640,128]{2,1,0:T(8,128)(2,1)S(1)}, u32[]{:S(2)}, u32[]{:S(2)}) async-start(bf16[8,640,128]{2,1,0:T(8,128)(2,1)} %shard_map.189), calls=%async_computation.1 | async-start | bytes 2621440 | tf_op jit(solution)/shard_map/all_to_all | solution.py:253
  73.2 2.1 %collective-permute-start = (bf16[8,512]{1,0:T(8,128)(2,1)S(1)}, bf16[8,512]{1,0:T(8,128)(2,1)S(1)}, u32[]{:S(2)}, u32[]{:S(2)}) collective-permute-start(bf16[8,512]{1,0:T(8,128)(2,1)S(1)} %get-tuple-element.18), channel_id=1, source_target_pairs={{0,16},{16,32},{32,48},{48,64},{64,80},{80,96},{96,112},{112,128},... | collective-permute-start | bytes 24584 | tf_op jit(solution)/shard_map/ppermute | solution.py:258
  75.3 0.0 copy-done.14
  75.3 0.1 copy.22.rate_ref
  75.4 1.2 collective-permute-done.rim_ref
  76.7 0.0 copy-done.3
  76.7 0.0 copy-done.4
  76.7 0.0 copy-done.5
  76.7 0.0 copy-done.7
  76.7 0.0 copy-done.8
  76.7 0.0 copy-done.9
  76.7 0.0 copy-done.10
  76.7 2.2 %shard_map.177 = (bf16[256,384]{1,0:T(8,128)(2,1)S(1)}, bf16[128,384]{1,0:T(8,128)(2,1)S(1)}, bf16[128,384]{1,0:T(8,128)(2,1)S(1)}, f32[4,384]{1,0:T(4,128)S(1)}...) custom-call(s32[1]{0:T(128)} %bitcast.group_ref, bf16[256,384]{1,0:T(8,128)(2,1)S(1)} %copy-done.3, ...), custom_call_target="tpu_custom_call" | custom-call | flops 2000000000 | bytes 1048576 | tf_op jit(solution)/shard_map/pallas_call | solution.py:44
  79.0 4.2 %collective-permute-start.1 = (bf16[272,128]{1,0:T(8,128)(2,1)S(1)}, bf16[272,128]{1,0:T(8,128)(2,1)S(1)}, u32[]{:S(2)}, u32[]{:S(2)}) collective-permute-start(bf16[272,128]{1,0:T(8,128)(2,1)S(1)} %get-tuple-element.24.own_ref), channel_id=1, source_target_pairs={{0,16},{16,32},{32,48},{48,0},{1,17},{17,33},{33,49},{49,1},{2,18}... | collective-permute-start | bytes 208904 | tf_op jit(solution)/shard_map/ppermute | solution.py:577
  83.2 4.7 %collective-permute-start.2 = (bf16[272,128]{1,0:T(8,128)(2,1)S(1)}, bf16[272,128]{1,0:T(8,128)(2,1)S(1)}, u32[]{:S(2)}, u32[]{:S(2)}) collective-permute-start(bf16[272,128]{1,0:T(8,128)(2,1)S(1)} %get-tuple-element.24.own_ref), channel_id=1, source_target_pairs={{0,32},{16,48},{32,0},{48,16},{1,33},{17,49},{33,1},{49,17},{2,34}... | collective-permute-start | bytes 208904 | tf_op jit(solution)/shard_map/ppermute | solution.py:577
  87.8 3.3 %collective-permute-start.3 = (bf16[272,128]{1,0:T(8,128)(2,1)S(1)}, bf16[272,128]{1,0:T(8,128)(2,1)S(1)}, u32[]{:S(2)}, u32[]{:S(2)}) collective-permute-start(bf16[272,128]{1,0:T(8,128)(2,1)S(1)} %get-tuple-element.24.own_ref), channel_id=1, source_target_pairs={{0,48},{16,0},{32,16},{48,32},{1,49},{17,1},{33,17},{49,33},{2,50}... | collective-permute-start | bytes 208904 | tf_op jit(solution)/shard_map/ppermute | solution.py:577
  91.1 0.0 collective-permute-done.1.first_ref
  91.1 0.0 collective-permute-done.2.second_ref
  91.2 2.9 %collective-permute-done.3.third_ref = bf16[272,128]{1,0:T(8,128)(2,1)S(1)} collective-permute-done((bf16[272,128]{1,0:T(8,128)(2,1)S(1)}, bf16[272,128]{1,0:T(8,128)(2,1)S(1)}, u32[]{:S(2)}, u32[]{:S(2)}) %collective-permute-start.3) | collective-permute-done | bytes 69664 | tf_op jit(solution)/shard_map/ppermute | solution.py:577
  94.0 0.1 shard_map.179
  94.2 0.0 copy-start.13
  94.2 4.3 %collective-permute-start.4 = (bf16[272,128]{1,0:T(8,128)(2,1)S(1)}, bf16[272,128]{1,0:T(8,128)(2,1)S(1)}, u32[]{:S(2)}, u32[]{:S(2)}) collective-permute-start(bf16[272,128]{1,0:T(8,128)(2,1)S(1)} %get-tuple-element.26), channel_id=1, source_target_pairs={{0,64},{64,128},{128,192},{192,256},{256,320},{320,384},{384,448},... | collective-permute-start | bytes 208904 | tf_op jit(solution)/shard_map/ppermute | solution.py:263
  98.4 2.8 %collective-permute-start.5 = (bf16[272,128]{1,0:T(8,128)(2,1)S(1)}, bf16[272,128]{1,0:T(8,128)(2,1)S(1)}, u32[]{:S(2)}, u32[]{:S(2)}) collective-permute-start(bf16[272,128]{1,0:T(8,128)(2,1)S(1)} %get-tuple-element.26), channel_id=1, source_target_pairs={{0,128},{64,192},{128,256},{192,320},{256,384},{320,448},{1,129},{... | collective-permute-start | bytes 208904 | tf_op jit(solution)/shard_map/ppermute | solution.py:263
  101.2 0.0 collective-permute-done.4.after_ref
  101.3 1.9 %collective-permute-done.5.before_ref = bf16[272,128]{1,0:T(8,128)(2,1)S(1)} collective-permute-done((bf16[272,128]{1,0:T(8,128)(2,1)S(1)}, bf16[272,128]{1,0:T(8,128)(2,1)S(1)}, u32[]{:S(2)}, u32[]{:S(2)}) %collective-permute-start.5) | collective-permute-done | bytes 69664 | tf_op jit(solution)/shard_map/ppermute | solution.py:263
  103.2 5.2 %collective-permute-start.6 = (bf16[272,128]{1,0:T(8,128)(2,1)S(1)}, bf16[272,128]{1,0:T(8,128)(2,1)S(1)}, u32[]{:S(2)}, u32[]{:S(2)}) collective-permute-start(bf16[272,128]{1,0:T(8,128)(2,1)S(1)} %shard_map.180.after_ref), channel_id=1, source_target_pairs={{0,128},{64,192},{128,256},{192,320},{256,384},{320,448},{1,129},{... | collective-permute-start | bytes 208904 | tf_op jit(solution)/shard_map/ppermute | solution.py:263
  108.4 0.0 all-to-all-done.1.parts_ref
  108.4 1.0 shard_map.190
  109.4 7.5 %all-to-all-start.2 = ((bf16[32,24,128]{2,1,0:T(8,128)(2,1)}), bf16[32,24,128]{2,1,0:T(8,128)(2,1)S(1)}, u32[]{:S(2)}, u32[]{:S(2)}) async-start(bf16[32,24,128]{2,1,0:T(8,128)(2,1)} %shard_map.190), calls=%async_computation.2 | async-start | bytes 393216 | tf_op jit(solution)/shard_map/all_to_all | solution.py:253
  117.0 0.1 copy.24.routes_ref
  117.1 0.1 copy.25.logit_ref
  117.2 0.1 copy.23.gain_ref
  117.4 0.0 collective-permute-done.6.before_ref
  117.4 0.0 copy-start.6
  117.4 7.7 %collective-permute-start.7 = (bf16[272,128]{1,0:T(8,128)(2,1)S(1)}, bf16[272,128]{1,0:T(8,128)(2,1)S(1)}, u32[]{:S(2)}, u32[]{:S(2)}) collective-permute-start(bf16[272,128]{1,0:T(8,128)(2,1)S(1)} %shard_map.181.after_ref), channel_id=1, source_target_pairs={{0,256},{64,320},{128,384},{192,448},{1,257},{65,321},{129,385},{1... | collective-permute-start | bytes 208904 | tf_op jit(solution)/shard_map/ppermute | solution.py:263
  125.2 0.6 shard_map.191.weight_ref
  125.8 0.8 shard_map.178.y_ref
  126.6 0.5 collective-permute-done.7.before_ref
  127.1 1.0 shard_map.183
  128.1 0.2 all-to-all-done.2.back_ref
  128.3 0.9 shard_map.192
  (14 shorter events, 0.1 us)
Async XLA Ops:
  3.0 50.4 %copy-start = (bf16[1,320,2048]{2,1,0:T(8,128)(2,1)S(1)}, bf16[1,320,2048]{2,1,0:T(8,128)(2,1)}, u32[]{:S(2)}) copy-start(bf16[1,320,2048]{2,1,0:T(8,128)(2,1)} %param.33) | copy-start | bytes 3932164
  3.0 53.2 %copy-start.2 = (bf16[1,2048,320]{1,2,0:T(8,128)(2,1)S(1)}, bf16[1,2048,320]{1,2,0:T(8,128)(2,1)}, u32[]{:S(2)}) copy-start(bf16[1,2048,320]{1,2,0:T(8,128)(2,1)} %param.32) | copy-start | bytes 3932164
  51.3 4.8 %copy-start.1 = (bf16[1,2048,320]{1,2,0:T(8,128)(2,1)S(1)}, bf16[1,2048,320]{1,2,0:T(8,128)(2,1)}, u32[]{:S(2)}) copy-start(bf16[1,2048,320]{1,2,0:T(8,128)(2,1)} %param.31) | copy-start | bytes 3932164
  51.3 6.6 %collective-permute-start.8 = (bf16[32,160,128]{2,1,0:T(8,128)(2,1)S(1)}, bf16[32,160,128]{2,1,0:T(8,128)(2,1)S(1)}, u32[]{:S(2)}, u32[]{:S(2)}) collective-permute-start(bf16[32,160,128]{2,1,0:T(8,128)(2,1)S(1)} %all_to_all.15.own_ref), channel_id=1, source_target_pairs={{0,1},{1,0},{2,3},{3,2},{4,5},{5,4},{6,7},{7,6},{8,9},{9,8},{10,11... | collective-permute-start | bytes 3932168 | tf_op jit(solution)/shard_map/ppermute | solution.py:271
  53.7 8.8 %collective-permute-start.10 = (bf16[320,1024]{1,0:T(8,128)(2,1)S(1)}, bf16[320,1024]{1,0:T(8,128)(2,1)S(1)}, u32[]{:S(2)}, u32[]{:S(2)}) collective-permute-start(bf16[320,1024]{1,0:T(8,128)(2,1)S(1)} %get-tuple-element.32), channel_id=1, source_target_pairs={{0,1},{1,0},{2,3},{3,2},{4,5},{5,4},{6,7},{7,6},{8,9},{9,8},{10,11... | collective-permute-start | bytes 1966088 | tf_op jit(solution)/shard_map/ppermute | solution.py:271
  59.8 3.8 %collective-permute-start.9 = (bf16[640,320]{1,0:T(8,128)(2,1)S(1)}, bf16[640,320]{1,0:T(8,128)(2,1)S(1)}, u32[]{:S(2)}, u32[]{:S(2)}) collective-permute-start(bf16[640,320]{1,0:T(8,128)(2,1)S(1)} %shard_map.186.hidden_ref), channel_id=1, source_target_pairs={{0,1},{1,0},{2,3},{3,2},{4,5},{5,4},{6,7},{7,6},{8,9},{9,8},{10,11... | collective-permute-start | bytes 1228808 | tf_op jit(solution)/shard_map/ppermute | solution.py:271
  65.5 9.9 %copy-start.14 = (f32[4]{0:T(128)S(1)}, f32[4]{0:T(128)}, u32[]{:S(2)}) copy-start(f32[4]{0:T(128)} %param.20) | copy-start | bytes 52
  65.5 11.2 %copy-start.3 = (bf16[256,384]{1,0:T(8,128)(2,1)S(1)}, bf16[256,384]{1,0:T(8,128)(2,1)}, u32[]{:S(2)}) copy-start(bf16[256,384]{1,0:T(8,128)(2,1)} %x_hbm.3) | copy-start | bytes 589828
  65.5 11.2 %copy-start.4 = (bf16[256,384]{1,0:T(8,128)(2,1)S(1)}, bf16[256,384]{1,0:T(8,128)(2,1)}, u32[]{:S(2)}) copy-start(bf16[256,384]{1,0:T(8,128)(2,1)} %b_hbm.3) | copy-start | bytes 589828
  65.5 11.2 %copy-start.5 = (bf16[256,384]{1,0:T(8,128)(2,1)S(1)}, bf16[256,384]{1,0:T(8,128)(2,1)}, u32[]{:S(2)}) copy-start(bf16[256,384]{1,0:T(8,128)(2,1)} %c_hbm.3) | copy-start | bytes 589828
  65.5 11.2 %copy-start.7 = (f32[4,384]{1,0:T(4,128)S(1)}, f32[4,384]{1,0:T(4,128)}, u32[]{:S(2)}) copy-start(f32[4,384]{1,0:T(4,128)} %dt_ref.1) | copy-start | bytes 18436
  65.5 11.2 %copy-start.8 = (f32[256,4]{0,1:T(4,128)S(1)}, f32[256,4]{0,1:T(4,128)}, u32[]{:S(2)}) copy-start(f32[256,4]{0,1:T(4,128)} %param.23) | copy-start | bytes 12292
  65.5 11.2 %copy-start.9 = (f32[256,4]{0,1:T(4,128)S(1)}, f32[256,4]{0,1:T(4,128)}, u32[]{:S(2)}) copy-start(f32[256,4]{0,1:T(4,128)} %param.24) | copy-start | bytes 12292
  65.5 11.2 %copy-start.10 = (f32[256,4]{0,1:T(4,128)S(1)}, f32[256,4]{0,1:T(4,128)}, u32[]{:S(2)}) copy-start(f32[256,4]{0,1:T(4,128)} %param.25) | copy-start | bytes 12292
  65.5 42.9 %all-to-all-start.1 = ((bf16[8,640,128]{2,1,0:T(8,128)(2,1)}), bf16[8,640,128]{2,1,0:T(8,128)(2,1)S(1)}, u32[]{:S(2)}, u32[]{:S(2)}) async-start(bf16[8,640,128]{2,1,0:T(8,128)(2,1)} %shard_map.189), calls=%async_computation.1 | async-start | bytes 2621440 | tf_op jit(solution)/shard_map/all_to_all | solution.py:253
  73.2 3.5 %collective-permute-start = (bf16[8,512]{1,0:T(8,128)(2,1)S(1)}, bf16[8,512]{1,0:T(8,128)(2,1)S(1)}, u32[]{:S(2)}, u32[]{:S(2)}) collective-permute-start(bf16[8,512]{1,0:T(8,128)(2,1)S(1)} %get-tuple-element.18), channel_id=1, source_target_pairs={{0,16},{16,32},{32,48},{48,64},{64,80},{80,96},{96,112},{112,128},... | collective-permute-start | bytes 24584 | tf_op jit(solution)/shard_map/ppermute | solution.py:258
  79.0 12.2 %collective-permute-start.1 = (bf16[272,128]{1,0:T(8,128)(2,1)S(1)}, bf16[272,128]{1,0:T(8,128)(2,1)S(1)}, u32[]{:S(2)}, u32[]{:S(2)}) collective-permute-start(bf16[272,128]{1,0:T(8,128)(2,1)S(1)} %get-tuple-element.24.own_ref), channel_id=1, source_target_pairs={{0,16},{16,32},{32,48},{48,0},{1,17},{17,33},{33,49},{49,1},{2,18}... | collective-permute-start | bytes 208904 | tf_op jit(solution)/shard_map/ppermute | solution.py:577
  83.2 8.0 %collective-permute-start.2 = (bf16[272,128]{1,0:T(8,128)(2,1)S(1)}, bf16[272,128]{1,0:T(8,128)(2,1)S(1)}, u32[]{:S(2)}, u32[]{:S(2)}) collective-permute-start(bf16[272,128]{1,0:T(8,128)(2,1)S(1)} %get-tuple-element.24.own_ref), channel_id=1, source_target_pairs={{0,32},{16,48},{32,0},{48,16},{1,33},{17,49},{33,1},{49,17},{2,34}... | collective-permute-start | bytes 208904 | tf_op jit(solution)/shard_map/ppermute | solution.py:577
  87.8 6.2 %collective-permute-start.3 = (bf16[272,128]{1,0:T(8,128)(2,1)S(1)}, bf16[272,128]{1,0:T(8,128)(2,1)S(1)}, u32[]{:S(2)}, u32[]{:S(2)}) collective-permute-start(bf16[272,128]{1,0:T(8,128)(2,1)S(1)} %get-tuple-element.24.own_ref), channel_id=1, source_target_pairs={{0,48},{16,0},{32,16},{48,32},{1,49},{17,1},{33,17},{49,33},{2,50}... | collective-permute-start | bytes 208904 | tf_op jit(solution)/shard_map/ppermute | solution.py:577
  94.0 22.9 %copy-start.11 = (s32[160,2]{0,1:T(2,128)S(1)}, s32[160,2]{0,1:T(2,128)}, u32[]{:S(2)}) copy-start(s32[160,2]{0,1:T(2,128)} %param.29) | copy-start | bytes 3844
  94.0 23.1 %copy-start.12 = (f32[160,2]{0,1:T(2,128)S(1)}, f32[160,2]{0,1:T(2,128)}, u32[]{:S(2)}) copy-start(f32[160,2]{0,1:T(2,128)} %param.30) | copy-start | bytes 3844
  94.2 23.0 %copy-start.13 = (f32[256]{0:T(256)S(1)}, f32[256]{0:T(256)}, u32[]{:S(2)}) copy-start(f32[256]{0:T(256)} %param.26) | copy-start | bytes 3076
  94.2 7.1 %collective-permute-start.4 = (bf16[272,128]{1,0:T(8,128)(2,1)S(1)}, bf16[272,128]{1,0:T(8,128)(2,1)S(1)}, u32[]{:S(2)}, u32[]{:S(2)}) collective-permute-start(bf16[272,128]{1,0:T(8,128)(2,1)S(1)} %get-tuple-element.26), channel_id=1, source_target_pairs={{0,64},{64,128},{128,192},{192,256},{256,320},{320,384},{384,448},... | collective-permute-start | bytes 208904 | tf_op jit(solution)/shard_map/ppermute | solution.py:263
  98.4 4.7 %collective-permute-start.5 = (bf16[272,128]{1,0:T(8,128)(2,1)S(1)}, bf16[272,128]{1,0:T(8,128)(2,1)S(1)}, u32[]{:S(2)}, u32[]{:S(2)}) collective-permute-start(bf16[272,128]{1,0:T(8,128)(2,1)S(1)} %get-tuple-element.26), channel_id=1, source_target_pairs={{0,128},{64,192},{128,256},{192,320},{256,384},{320,448},{1,129},{... | collective-permute-start | bytes 208904 | tf_op jit(solution)/shard_map/ppermute | solution.py:263
  103.2 14.2 %collective-permute-start.6 = (bf16[272,128]{1,0:T(8,128)(2,1)S(1)}, bf16[272,128]{1,0:T(8,128)(2,1)S(1)}, u32[]{:S(2)}, u32[]{:S(2)}) collective-permute-start(bf16[272,128]{1,0:T(8,128)(2,1)S(1)} %shard_map.180.after_ref), channel_id=1, source_target_pairs={{0,128},{64,192},{128,256},{192,320},{256,384},{320,448},{1,129},{... | collective-permute-start | bytes 208904 | tf_op jit(solution)/shard_map/ppermute | solution.py:263
  109.4 18.9 %all-to-all-start.2 = ((bf16[32,24,128]{2,1,0:T(8,128)(2,1)}), bf16[32,24,128]{2,1,0:T(8,128)(2,1)S(1)}, u32[]{:S(2)}, u32[]{:S(2)}) async-start(bf16[32,24,128]{2,1,0:T(8,128)(2,1)} %shard_map.190), calls=%async_computation.2 | async-start | bytes 393216 | tf_op jit(solution)/shard_map/all_to_all | solution.py:253
  117.4 9.7 %copy-start.6 = (bf16[256,384]{1,0:T(8,128)(2,1)S(1)}, bf16[256,384]{1,0:T(8,128)(2,1)}, u32[]{:S(2)}) copy-start(bf16[256,384]{1,0:T(8,128)(2,1)} %z_ref.1) | copy-start | bytes 589828
  117.4 9.7 %collective-permute-start.7 = (bf16[272,128]{1,0:T(8,128)(2,1)S(1)}, bf16[272,128]{1,0:T(8,128)(2,1)S(1)}, u32[]{:S(2)}, u32[]{:S(2)}) collective-permute-start(bf16[272,128]{1,0:T(8,128)(2,1)S(1)} %shard_map.181.after_ref), channel_id=1, source_target_pairs={{0,256},{64,320},{128,384},{192,448},{1,257},{65,321},{129,385},{1... | collective-permute-start | bytes 208904 | tf_op jit(solution)/shard_map/ppermute | solution.py:263

commit v4 on v3

--- a/solution.py
+++ b/solution.py
@@ -37,15 +37,16 @@
     return jnp.dot(a, b, preferred_element_type=F32)
 
 
-def call(kernel, out_shape, args, flops, smem=0, hbm=0, vmem=8, scratch=()):
+def call(kernel, out_shape, args, flops, smem=0, hbm=0, out_hbm=False, vmem=8, scratch=()):
     specs = [pl.BlockSpec(memory_space=pltpu.SMEM)] * smem
     specs += [pl.BlockSpec(memory_space=pltpu.HBM)] * hbm
     specs += [pl.BlockSpec(memory_space=pltpu.VMEM)] * (len(args) - smem - hbm)
+    out_space = pltpu.HBM if out_hbm else pltpu.VMEM
     return pl.pallas_call(
         kernel,
         out_shape=out_shape,
         in_specs=specs,
-        out_specs=jax.tree.map(lambda _: pl.BlockSpec(memory_space=pltpu.VMEM), out_shape),
+        out_specs=jax.tree.map(lambda _: pl.BlockSpec(memory_space=out_space), out_shape),
         scratch_shapes=scratch,
         compiler_params=pltpu.CompilerParams(vmem_limit_bytes=vmem * MIB),
         cost_estimate=pl.CostEstimate(flops=flops, bytes_accessed=1 << 20, transcendentals=0),
@@ -66,13 +67,6 @@
         copy.wait()
 
 
-def store_main(ref, value):
-    for j in range(N_BLK):
-        ref[:, HEAD_ROWS * j : HEAD_ROWS * (j + 1), :] = value[
-            :, LANES * j : LANES * (j + 1)
-        ].reshape(N_EXP, HEAD_ROWS, LANES)
-
-
 def store_tail(ref, value):
     for g in range(2):
         low = N_BLK * HEAD_ROWS + HEAD_ROWS * g
@@ -99,7 +93,7 @@
     return jnp.concatenate(parts, axis=1)
 
 
-def prep_kernel(core_ref, rows_ref, gain_ref, routes_ref, out_ref):
+def prep_kernel(core_ref, rows_ref, gain_ref, routes_ref, out_hbm, out_ref, sems):
     tokens, features = rows_ref.shape
     half = features // 2
     low = pl.multiple_of(core_ref[0] * half, half)
@@ -113,17 +107,40 @@
     before = (iota((tokens, tokens), 0) < iota((tokens, tokens), 1)).astype(BF16)
     ranks = dot((picks[0] + picks[1]).astype(BF16), before)
     row = iota((N_EXP * HEAD_ROWS, tokens), 0)
-    main = jnp.zeros((N_EXP * HEAD_ROWS, tokens), F32)
-    tails = [jnp.zeros((N_EXP * HEAD_ROWS, tokens), F32) for _ in range(TAIL_ROWS)]
+    places = []
     for k in range(2):
         rank = jnp.sum(ranks * picks[k], axis=0, keepdims=True).astype(jnp.int32)
         start = routes[k : k + 1, :] * HEAD_ROWS
-        in_main = jnp.where(rank < HEAD_ROWS, start + rank, -1)
-        in_tail = jnp.where(rank >= HEAD_ROWS, start + rank - HEAD_ROWS, -1000)
-        main = main + (row == in_main).astype(F32)
-        for q in range(4):
-            tails[q] = tails[q] + (row == in_tail + TAIL_ROWS * q).astype(F32)
-    store_main(out_ref, dot(main.astype(BF16), normed).astype(BF16))
+        places.append(
+            (
+                jnp.where(rank < HEAD_ROWS, start + rank, -1),
+                jnp.where(rank >= HEAD_ROWS, start + rank - HEAD_ROWS, -1000),
+            )
+        )
+
+    def one_hot(first, second):
+        return jnp.where((row == first) | (row == second), 1.0, 0.0)
+
+    main = one_hot(places[0][0], places[1][0])
+    tails = [
+        one_hot(places[0][1] + TAIL_ROWS * q, places[1][1] + TAIL_ROWS * q) for q in range(4)
+    ]
+    main = main.astype(BF16)
+    copies = []
+
+    def send(k, low, size):
+        part = pl.ds(low, size)
+        copies.append(pltpu.make_async_copy(out_ref.at[:, part], out_hbm.at[:, part], sems.at[k]))
+        copies[-1].start()
+
+    for g in range(4):
+        value = dot(main, normed[:, 2 * LANES * g : 2 * LANES * (g + 1)]).astype(BF16)
+        for b in range(2):
+            low = HEAD_ROWS * (2 * g + b)
+            out_ref[:, low : low + HEAD_ROWS, :] = value[:, LANES * b : LANES * (b + 1)].reshape(
+                N_EXP, HEAD_ROWS, LANES
+            )
+        send(g, 2 * HEAD_ROWS * g, 2 * HEAD_ROWS)
     tail = jnp.zeros((N_EXP * HEAD_ROWS, 2 * LANES), F32)
     for q in range(4):
         pair = jnp.concatenate(
@@ -135,6 +152,9 @@
         )
         tail = tail + dot(tails[q].astype(BF16), pair)
     store_tail(out_ref, tail.astype(BF16))
+    send(4, N_BLK * HEAD_ROWS, 2 * HEAD_ROWS)
+    for copy in copies:
+        copy.wait()
 
 
 def tail_pick(q):
@@ -153,12 +173,15 @@
     return jnp.concatenate([load_main(ref), tail], axis=0)
 
 
-def first_half_kernel(core_ref, own_ref, gate_ref, up_ref, gate_out, up_out):
+def first_half_kernel(core_ref, up_hbm, own_ref, gate_ref, gate_out, up_out, up_ref, sem):
     half = gate_ref.shape[1] // 2
     low = pl.multiple_of(core_ref[0] * half, half)
+    copy = pltpu.make_async_copy(up_hbm.at[:, pl.ds(low, half)], up_ref, sem)
+    copy.start()
     rows = unpacked(own_ref)
     gate_out[...] = over_last(rows, gate_ref[:, pl.ds(low, half)])
-    up_out[...] = over_last(rows, up_ref[:, pl.ds(low, half)])
+    copy.wait()
+    up_out[...] = over_last(rows, up_ref[...])
 
 
 def down_columns(down_ref, parity):
@@ -191,10 +214,18 @@
     out_ref[...] = dot(hidden_ref[...], down_ref[...])
 
 
-def other_down_kernel(hidden_ref, down_ref, own_ref, out_ref):
-    value = own_ref[...] + dot(hidden_ref[...], down_ref[...])
-    for j in range(N_BLK):
-        out_ref[j] = value[:, LANES * j : LANES * (j + 1)].astype(BF16)
+def other_down_kernel(hidden_ref, down_ref, own_ref, out_hbm, out_ref, sems):
+    copies = []
+    for g in range(4):
+        columns = slice(2 * LANES * g, 2 * LANES * (g + 1))
+        value = own_ref[:, columns] + dot(hidden_ref[...], down_ref[:, columns])
+        out_ref[2 * g] = value[:, :LANES].astype(BF16)
+        out_ref[2 * g + 1] = value[:, LANES:].astype(BF16)
+        pair = pl.ds(2 * g, 2)
+        copies.append(pltpu.make_async_copy(out_ref.at[pair], out_hbm.at[pair], sems.at[g]))
+        copies[-1].start()
+    for copy in copies:
+        copy.wait()
 
 
 def collect_kernel(parts_ref, out_ref):
@@ -307,7 +338,14 @@
     other = swap_cores(own)
     half_act = sds((rows, hidden_units), F32)
     gate_act, up_act = call(
-        first_half_kernel, (half_act, half_act), (core, own, gate, up), 10**9, smem=1, vmem=20
+        first_half_kernel,
+        (half_act, half_act),
+        (core, *in_hbm(up), own, gate),
+        10**9,
+        smem=1,
+        hbm=1,
+        vmem=20,
+        scratch=(pltpu.VMEM((up.shape[0], up.shape[1] // 2), BF16), pltpu.SemaphoreType.DMA),
     )
     hidden = call(
         second_half_kernel,
@@ -330,7 +368,9 @@
         sds((N_BLK, rows, LANES), BF16),
         (partner, down_other, mine),
         6 * 10**8,
+        out_hbm=True,
         vmem=12,
+        scratch=(pltpu.VMEM((N_BLK, rows, LANES), BF16), pltpu.SemaphoreType.DMA((4,))),
     )
 
 
@@ -546,7 +586,15 @@
     group = group.astype(jnp.int32)[None]
     own_rim, *tokens = first_loads(group, x_in, b_in, c_in, moe_rows, moe_gain, routes)
     rims = from_behind(own_rim, 1)
-    outbox = call(prep_kernel, sds((N_EXP, CHUNK, LANES), BF16), (core, *tokens), 5 * 10**8, smem=1)
+    outbox = call(
+        prep_kernel,
+        sds((N_EXP, CHUNK, LANES), BF16),
+        (core, *tokens),
+        5 * 10**8,
+        smem=1,
+        out_hbm=True,
+        scratch=(pltpu.VMEM((N_EXP, CHUNK, LANES), BF16), pltpu.SemaphoreType.DMA((5,))),
+    )
     arrived = exchange(outbox, EP)
     down_parts = down_halves(core, w_down[0])
     x_conv, b_conv, c_conv, cum, step_dt, sent = call(

time: 130 us -> 132 us (1.015)
  Pallas kernels: 15.7 us -> 17.5 us
    pallas_call x17, Pallas kernels: 15.7 us -> 17.5 us  [call(): pl.pallas_call(kernel, out_shape=out_shape, in_specs=specs, out_specs=jax...]
where the time goes in v4:
time: 132 us; the launch traced here: 131 us
  starting transfers between devices  55.9 us (42%)
  blocking collectives  48.3 us (37%)
  Pallas kernels  17.5 us (13%)
  waiting for transfers between devices  7.73 us (6%)
    all_to_all x1, blocking collectives, exchange(): return lax.all_to_all(value, axes, split_axis=0, concat_axis=0, tiled=True)  48.3 us
    ppermute x4, starting transfers between devices, rows_behind(): lax.ppermute(value, 'z', [(k, k + steps) for k in range(count - steps)])  20 us
    pallas_call x17, Pallas kernels, call(): pl.pallas_call(kernel, out_shape=out_shape, in_specs=specs, out_specs=jax...  17.5 us
    all_to_all x2, starting transfers between devices, exchange(): return lax.all_to_all(value, axes, split_axis=0, concat_axis=0, tiled=True)  15.2 us
    ppermute x3, starting transfers between devices, on_device(): lax.ppermute(sent, 'x', [(k, (k + step) % 4) for k in range(4)])  12.2 us
    ppermute x3, starting transfers between devices, swap_cores(): return lax.ppermute(value, 'c', [(0, 1), (1, 0)])  6.37 us
    ppermute x3, waiting for transfers between devices, on_device(): lax.ppermute(sent, 'x', [(k, (k + step) % 4) for k in range(4)])  2.87 us
  transfers between devices with their start and end apart: 13, of which 6 were waited for; matrix products, arithmetic and copies ran while one was open for 0% of the time, Pallas kernels for 8%

profile of v4, /device:TPU:8, one launch (start us, length us, event | category | flops | bytes accessed | tf_op | source)
XLA Modules:
  0.0 131.0 jit_solution(6684979600854271332)
XLA Ops:
  0.6 1.2 shard_map.176
  1.9 2.6 %shard_map.184 = bf16[32,160,128]{2,1,0:T(8,128)(2,1)S(1)} custom-call(s32[1]{0:T(128)} %bitcast.9.core_ref, bf16[160,2048]{1,0:T(8,128)(2,1)S(1)} %get-tuple-element.27.rows_ref, f32[1,2048]{1,0:T(1,128)S(1)} %get-tuple-element.28.gain_ref, s32[2,160]{1,0:T(2,128)S(1)} %get-tuple-element.29.routes_ref), custom_call_target="tpu_custom_call" | custom-call | flops 500000000 | bytes 1048576 | tf_op jit(solution)/shard_map/pallas_call | solution.py:45
  4.5 0.0 copy-start
  4.5 48.3 %all_to_all.15.own_ref = bf16[32,160,128]{2,1,0:T(8,128)(2,1)S(1)} all-to-all(bf16[32,160,128]{2,1,0:T(8,128)(2,1)S(1)} %shard_map.184), channel_id=1, replica_groups=mesh['z'=8,'x'=4,'y'=8,'c'=2] {'z','x'}, dimensions={0} | all-to-all | bytes 2621440 | tf_op jit(solution)/shard_map/all_to_all | solution.py:284
  52.9 2.0 %collective-permute-start.8 = (bf16[32,160,128]{2,1,0:T(8,128)(2,1)S(1)}, bf16[32,160,128]{2,1,0:T(8,128)(2,1)S(1)}, u32[]{:S(2)}, u32[]{:S(2)}) collective-permute-start(bf16[32,160,128]{2,1,0:T(8,128)(2,1)S(1)} %all_to_all.15.own_ref), channel_id=1, source_target_pairs={{0,1},{1,0},{2,3},{3,2},{4,5},{5,4},{6,7},{7,6},{8,9},{9,8},{10,11... | collective-permute-start | bytes 3932168 | tf_op jit(solution)/shard_map/ppermute | solution.py:302
  54.9 0.0 copy-done
  54.9 0.3 shard_map.187
  55.3 2.4 %collective-permute-start.10 = (bf16[320,1024]{1,0:T(8,128)(2,1)S(1)}, bf16[320,1024]{1,0:T(8,128)(2,1)S(1)}, u32[]{:S(2)}, u32[]{:S(2)}) collective-permute-start(bf16[320,1024]{1,0:T(8,128)(2,1)S(1)} %get-tuple-element.32), channel_id=1, source_target_pairs={{0,1},{1,0},{2,3},{3,2},{4,5},{5,4},{6,7},{7,6},{8,9},{9,8},{10,11... | collective-permute-start | bytes 1966088 | tf_op jit(solution)/shard_map/ppermute | solution.py:302
  57.7 0.0 copy-done.1
  57.7 0.0 copy-start.2
  57.7 2.1 %shard_map.185 = (f32[640,320]{1,0:T(8,128)S(1)}, f32[640,320]{1,0:T(8,128)S(1)}) custom-call(s32[1]{0:T(128)} %bitcast.9.core_ref, bf16[320,2048]{1,0:T(8,128)(2,1)} %bitcast.21, bf16[32,160,128]{2,1,0:T(8,128)(2,1)S(1)} %all_to_all.15.own_ref, bf16[320,2048]{1,0:T(8,128)(2,1)S(1)} %bitcast.19), custom_call_target="tpu_custom_call" | custom-call | flops 1000000000 | bytes 1048576 | tf_op jit(solution)/shard_map/pallas_call | solution.py:45
  59.8 0.0 collective-permute-done.8.other_ref
  59.8 0.0 copy-done.2
  59.8 1.8 %shard_map.186.hidden_ref = bf16[640,320]{1,0:T(8,128)(2,1)S(1)} custom-call(s32[1]{0:T(128)} %bitcast.9.core_ref, bf16[32,160,128]{2,1,0:T(8,128)(2,1)S(1)} %collective-permute-done.8.other_ref, bf16[320,2048]{1,0:T(8,128)(2,1)S(1)} %bitcast.20, bf16[320,2048]{1,0:T(8,128)(2,1)S(1)} %bitcast.22, f32[640,320]{1,0:T(8,128)S(1)} %get-tuple-element.30.gate_in, ...), custom_call_target="tpu_custom_call" | custom-call | flops 2000000000 | bytes 1048576 | tf_op jit(solution)/shard_map/pallas_call | solution.py:45
  61.7 1.9 %collective-permute-start.9 = (bf16[640,320]{1,0:T(8,128)(2,1)S(1)}, bf16[640,320]{1,0:T(8,128)(2,1)S(1)}, u32[]{:S(2)}, u32[]{:S(2)}) collective-permute-start(bf16[640,320]{1,0:T(8,128)(2,1)S(1)} %shard_map.186.hidden_ref), channel_id=1, source_target_pairs={{0,1},{1,0},{2,3},{3,2},{4,5},{5,4},{6,7},{7,6},{8,9},{9,8},{10,11... | collective-permute-start | bytes 1228808 | tf_op jit(solution)/shard_map/ppermute | solution.py:302
  63.6 0.8 shard_map.188.own_ref
  64.4 0.0 collective-permute-done.10.down_ref
  64.4 1.0 collective-permute-done.9.hidden_ref
  65.4 1.8 %shard_map.189 = bf16[8,640,128]{2,1,0:T(8,128)(2,1)} custom-call(bf16[640,320]{1,0:T(8,128)(2,1)S(1)} %collective-permute-done.9.hidden_ref, bf16[320,1024]{1,0:T(8,128)(2,1)S(1)} %collective-permute-done.10.down_ref, f32[640,1024]{1,0:T(8,128)S(1)} %shard_map.188.own_ref), custom_call_target="tpu_custom_call" | custom-call | flops 600000000 | bytes 1048576 | tf_op jit(solution)/shard_map/pallas_call | solution.py:45
  67.2 0.0 copy-start.14
  67.2 0.0 copy-start.3
  67.2 0.0 copy-start.4
  67.3 0.0 copy-start.5
  67.3 0.0 copy-start.7
  67.3 0.0 copy-start.8
  67.3 0.0 copy-start.9
  67.3 0.0 copy-start.10
  67.3 7.7 %all-to-all-start.1 = ((bf16[8,640,128]{2,1,0:T(8,128)(2,1)}), bf16[8,640,128]{2,1,0:T(8,128)(2,1)S(1)}, u32[]{:S(2)}, u32[]{:S(2)}) async-start(bf16[8,640,128]{2,1,0:T(8,128)(2,1)} %shard_map.189), calls=%async_computation.1 | async-start | bytes 2621440 | tf_op jit(solution)/shard_map/all_to_all | solution.py:284
  75.0 2.1 %collective-permute-start = (bf16[8,512]{1,0:T(8,128)(2,1)S(1)}, bf16[8,512]{1,0:T(8,128)(2,1)S(1)}, u32[]{:S(2)}, u32[]{:S(2)}) collective-permute-start(bf16[8,512]{1,0:T(8,128)(2,1)S(1)} %get-tuple-element.18), channel_id=1, source_target_pairs={{0,16},{16,32},{32,48},{48,64},{64,80},{80,96},{96,112},{112,128},... | collective-permute-start | bytes 24584 | tf_op jit(solution)/shard_map/ppermute | solution.py:289
  77.1 0.0 copy-done.14
  77.1 0.1 copy.22.rate_ref
  77.2 1.2 collective-permute-done.rim_ref
  78.5 0.0 copy-done.3
  78.5 0.0 copy-done.4
  78.5 0.0 copy-done.5
  78.5 2.2 %shard_map.177 = (bf16[256,384]{1,0:T(8,128)(2,1)S(1)}, bf16[128,384]{1,0:T(8,128)(2,1)S(1)}, bf16[128,384]{1,0:T(8,128)(2,1)S(1)}, f32[4,384]{1,0:T(4,128)S(1)}...) custom-call(s32[1]{0:T(128)} %bitcast.group_ref, bf16[256,384]{1,0:T(8,128)(2,1)S(1)} %copy-done.3, ...), custom_call_target="tpu_custom_call" | custom-call | flops 2000000000 | bytes 1048576 | tf_op jit(solution)/shard_map/pallas_call | solution.py:45
  80.7 4.2 %collective-permute-start.1 = (bf16[272,128]{1,0:T(8,128)(2,1)S(1)}, bf16[272,128]{1,0:T(8,128)(2,1)S(1)}, u32[]{:S(2)}, u32[]{:S(2)}) collective-permute-start(bf16[272,128]{1,0:T(8,128)(2,1)S(1)} %get-tuple-element.24.own_ref), channel_id=1, source_target_pairs={{0,16},{16,32},{32,48},{48,0},{1,17},{17,33},{33,49},{49,1},{2,18}... | collective-permute-start | bytes 208904 | tf_op jit(solution)/shard_map/ppermute | solution.py:625
  85.0 4.7 %collective-permute-start.2 = (bf16[272,128]{1,0:T(8,128)(2,1)S(1)}, bf16[272,128]{1,0:T(8,128)(2,1)S(1)}, u32[]{:S(2)}, u32[]{:S(2)}) collective-permute-start(bf16[272,128]{1,0:T(8,128)(2,1)S(1)} %get-tuple-element.24.own_ref), channel_id=1, source_target_pairs={{0,32},{16,48},{32,0},{48,16},{1,33},{17,49},{33,1},{49,17},{2,34}... | collective-permute-start | bytes 208904 | tf_op jit(solution)/shard_map/ppermute | solution.py:625
  89.6 3.3 %collective-permute-start.3 = (bf16[272,128]{1,0:T(8,128)(2,1)S(1)}, bf16[272,128]{1,0:T(8,128)(2,1)S(1)}, u32[]{:S(2)}, u32[]{:S(2)}) collective-permute-start(bf16[272,128]{1,0:T(8,128)(2,1)S(1)} %get-tuple-element.24.own_ref), channel_id=1, source_target_pairs={{0,48},{16,0},{32,16},{48,32},{1,49},{17,1},{33,17},{49,33},{2,50}... | collective-permute-start | bytes 208904 | tf_op jit(solution)/shard_map/ppermute | solution.py:625
  92.9 0.0 collective-permute-done.1.first_ref
  92.9 0.0 collective-permute-done.2.second_ref
  92.9 2.9 %collective-permute-done.3.third_ref = bf16[272,128]{1,0:T(8,128)(2,1)S(1)} collective-permute-done((bf16[272,128]{1,0:T(8,128)(2,1)S(1)}, bf16[272,128]{1,0:T(8,128)(2,1)S(1)}, u32[]{:S(2)}, u32[]{:S(2)}) %collective-permute-start.3) | collective-permute-done | bytes 69664 | tf_op jit(solution)/shard_map/ppermute | solution.py:625
  95.8 0.1 shard_map.179
  96.0 0.0 copy-start.13
  96.0 4.3 %collective-permute-start.4 = (bf16[272,128]{1,0:T(8,128)(2,1)S(1)}, bf16[272,128]{1,0:T(8,128)(2,1)S(1)}, u32[]{:S(2)}, u32[]{:S(2)}) collective-permute-start(bf16[272,128]{1,0:T(8,128)(2,1)S(1)} %get-tuple-element.26), channel_id=1, source_target_pairs={{0,64},{64,128},{128,192},{192,256},{256,320},{320,384},{384,448},... | collective-permute-start | bytes 208904 | tf_op jit(solution)/shard_map/ppermute | solution.py:294
  100.2 2.8 %collective-permute-start.5 = (bf16[272,128]{1,0:T(8,128)(2,1)S(1)}, bf16[272,128]{1,0:T(8,128)(2,1)S(1)}, u32[]{:S(2)}, u32[]{:S(2)}) collective-permute-start(bf16[272,128]{1,0:T(8,128)(2,1)S(1)} %get-tuple-element.26), channel_id=1, source_target_pairs={{0,128},{64,192},{128,256},{192,320},{256,384},{320,448},{1,129},{... | collective-permute-start | bytes 208904 | tf_op jit(solution)/shard_map/ppermute | solution.py:294
  103.0 0.0 collective-permute-done.4.after_ref
  103.0 1.9 %collective-permute-done.5.before_ref = bf16[272,128]{1,0:T(8,128)(2,1)S(1)} collective-permute-done((bf16[272,128]{1,0:T(8,128)(2,1)S(1)}, bf16[272,128]{1,0:T(8,128)(2,1)S(1)}, u32[]{:S(2)}, u32[]{:S(2)}) %collective-permute-start.5) | collective-permute-done | bytes 69664 | tf_op jit(solution)/shard_map/ppermute | solution.py:294
  105.0 5.2 %collective-permute-start.6 = (bf16[272,128]{1,0:T(8,128)(2,1)S(1)}, bf16[272,128]{1,0:T(8,128)(2,1)S(1)}, u32[]{:S(2)}, u32[]{:S(2)}) collective-permute-start(bf16[272,128]{1,0:T(8,128)(2,1)S(1)} %shard_map.180.after_ref), channel_id=1, source_target_pairs={{0,128},{64,192},{128,256},{192,320},{256,384},{320,448},{1,129},{... | collective-permute-start | bytes 208904 | tf_op jit(solution)/shard_map/ppermute | solution.py:294
  110.2 0.0 all-to-all-done.1.parts_ref
  110.2 1.0 shard_map.190
  111.2 7.5 %all-to-all-start.2 = ((bf16[32,24,128]{2,1,0:T(8,128)(2,1)}), bf16[32,24,128]{2,1,0:T(8,128)(2,1)S(1)}, u32[]{:S(2)}, u32[]{:S(2)}) async-start(bf16[32,24,128]{2,1,0:T(8,128)(2,1)} %shard_map.190), calls=%async_computation.2 | async-start | bytes 393216 | tf_op jit(solution)/shard_map/all_to_all | solution.py:284
  118.8 0.1 copy.24.routes_ref
  118.9 0.1 copy.25.logit_ref
  119.0 0.1 copy.23.gain_ref
  119.2 0.0 collective-permute-done.6.before_ref
  119.2 0.0 copy-start.6
  119.2 7.7 %collective-permute-start.7 = (bf16[272,128]{1,0:T(8,128)(2,1)S(1)}, bf16[272,128]{1,0:T(8,128)(2,1)S(1)}, u32[]{:S(2)}, u32[]{:S(2)}) collective-permute-start(bf16[272,128]{1,0:T(8,128)(2,1)S(1)} %shard_map.181.after_ref), channel_id=1, source_target_pairs={{0,256},{64,320},{128,384},{192,448},{1,257},{65,321},{129,385},{1... | collective-permute-start | bytes 208904 | tf_op jit(solution)/shard_map/ppermute | solution.py:294
  127.0 0.6 shard_map.191.weight_ref
  127.6 0.8 shard_map.178.y_ref
  128.4 0.5 collective-permute-done.7.before_ref
  128.9 1.0 shard_map.183
  129.9 0.2 all-to-all-done.2.back_ref
  130.1 0.9 shard_map.192
  (14 shorter events, 0.1 us)
Async XLA Ops:
  4.5 50.4 %copy-start = (bf16[1,320,2048]{2,1,0:T(8,128)(2,1)S(1)}, bf16[1,320,2048]{2,1,0:T(8,128)(2,1)}, u32[]{:S(2)}) copy-start(bf16[1,320,2048]{2,1,0:T(8,128)(2,1)} %param.33) | copy-start | bytes 3932164
  52.8 4.8 %copy-start.1 = (bf16[1,2048,320]{1,2,0:T(8,128)(2,1)S(1)}, bf16[1,2048,320]{1,2,0:T(8,128)(2,1)}, u32[]{:S(2)}) copy-start(bf16[1,2048,320]{1,2,0:T(8,128)(2,1)} %param.31) | copy-start | bytes 3932164
  52.9 6.9 %collective-permute-start.8 = (bf16[32,160,128]{2,1,0:T(8,128)(2,1)S(1)}, bf16[32,160,128]{2,1,0:T(8,128)(2,1)S(1)}, u32[]{:S(2)}, u32[]{:S(2)}) collective-permute-start(bf16[32,160,128]{2,1,0:T(8,128)(2,1)S(1)} %all_to_all.15.own_ref), channel_id=1, source_target_pairs={{0,1},{1,0},{2,3},{3,2},{4,5},{5,4},{6,7},{7,6},{8,9},{9,8},{10,11... | collective-permute-start | bytes 3932168 | tf_op jit(solution)/shard_map/ppermute | solution.py:302
  55.3 9.2 %collective-permute-start.10 = (bf16[320,1024]{1,0:T(8,128)(2,1)S(1)}, bf16[320,1024]{1,0:T(8,128)(2,1)S(1)}, u32[]{:S(2)}, u32[]{:S(2)}) collective-permute-start(bf16[320,1024]{1,0:T(8,128)(2,1)S(1)} %get-tuple-element.32), channel_id=1, source_target_pairs={{0,1},{1,0},{2,3},{3,2},{4,5},{5,4},{6,7},{7,6},{8,9},{9,8},{10,11... | collective-permute-start | bytes 1966088 | tf_op jit(solution)/shard_map/ppermute | solution.py:302
  57.7 2.1 %copy-start.2 = (bf16[1,2048,320]{1,2,0:T(8,128)(2,1)S(1)}, bf16[1,2048,320]{1,2,0:T(8,128)(2,1)}, u32[]{:S(2)}) copy-start(bf16[1,2048,320]{1,2,0:T(8,128)(2,1)} %param.32) | copy-start | bytes 3932164
  61.7 3.8 %collective-permute-start.9 = (bf16[640,320]{1,0:T(8,128)(2,1)S(1)}, bf16[640,320]{1,0:T(8,128)(2,1)S(1)}, u32[]{:S(2)}, u32[]{:S(2)}) collective-permute-start(bf16[640,320]{1,0:T(8,128)(2,1)S(1)} %shard_map.186.hidden_ref), channel_id=1, source_target_pairs={{0,1},{1,0},{2,3},{3,2},{4,5},{5,4},{6,7},{7,6},{8,9},{9,8},{10,11... | collective-permute-start | bytes 1228808 | tf_op jit(solution)/shard_map/ppermute | solution.py:302
  67.2 9.9 %copy-start.14 = (f32[4]{0:T(128)S(1)}, f32[4]{0:T(128)}, u32[]{:S(2)}) copy-start(f32[4]{0:T(128)} %param.20) | copy-start | bytes 52
  67.2 11.3 %copy-start.3 = (bf16[256,384]{1,0:T(8,128)(2,1)S(1)}, bf16[256,384]{1,0:T(8,128)(2,1)}, u32[]{:S(2)}) copy-start(bf16[256,384]{1,0:T(8,128)(2,1)} %x_hbm.3) | copy-start | bytes 589828
  67.2 11.2 %copy-start.4 = (bf16[256,384]{1,0:T(8,128)(2,1)S(1)}, bf16[256,384]{1,0:T(8,128)(2,1)}, u32[]{:S(2)}) copy-start(bf16[256,384]{1,0:T(8,128)(2,1)} %b_hbm.3) | copy-start | bytes 589828
  67.3 11.2 %copy-start.5 = (bf16[256,384]{1,0:T(8,128)(2,1)S(1)}, bf16[256,384]{1,0:T(8,128)(2,1)}, u32[]{:S(2)}) copy-start(bf16[256,384]{1,0:T(8,128)(2,1)} %c_hbm.3) | copy-start | bytes 589828
  67.3 11.2 %copy-start.7 = (f32[4,384]{1,0:T(4,128)S(1)}, f32[4,384]{1,0:T(4,128)}, u32[]{:S(2)}) copy-start(f32[4,384]{1,0:T(4,128)} %dt_ref.1) | copy-start | bytes 18436
  67.3 11.2 %copy-start.8 = (f32[256,4]{0,1:T(4,128)S(1)}, f32[256,4]{0,1:T(4,128)}, u32[]{:S(2)}) copy-start(f32[256,4]{0,1:T(4,128)} %param.23) | copy-start | bytes 12292
  67.3 11.2 %copy-start.9 = (f32[256,4]{0,1:T(4,128)S(1)}, f32[256,4]{0,1:T(4,128)}, u32[]{:S(2)}) copy-start(f32[256,4]{0,1:T(4,128)} %param.24) | copy-start | bytes 12292
  67.3 11.2 %copy-start.10 = (f32[256,4]{0,1:T(4,128)S(1)}, f32[256,4]{0,1:T(4,128)}, u32[]{:S(2)}) copy-start(f32[256,4]{0,1:T(4,128)} %param.25) | copy-start | bytes 12292
  67.3 42.9 %all-to-all-start.1 = ((bf16[8,640,128]{2,1,0:T(8,128)(2,1)}), bf16[8,640,128]{2,1,0:T(8,128)(2,1)S(1)}, u32[]{:S(2)}, u32[]{:S(2)}) async-start(bf16[8,640,128]{2,1,0:T(8,128)(2,1)} %shard_map.189), calls=%async_computation.1 | async-start | bytes 2621440 | tf_op jit(solution)/shard_map/all_to_all | solution.py:284
  75.0 3.5 %collective-permute-start = (bf16[8,512]{1,0:T(8,128)(2,1)S(1)}, bf16[8,512]{1,0:T(8,128)(2,1)S(1)}, u32[]{:S(2)}, u32[]{:S(2)}) collective-permute-start(bf16[8,512]{1,0:T(8,128)(2,1)S(1)} %get-tuple-element.18), channel_id=1, source_target_pairs={{0,16},{16,32},{32,48},{48,64},{64,80},{80,96},{96,112},{112,128},... | collective-permute-start | bytes 24584 | tf_op jit(solution)/shard_map/ppermute | solution.py:289
  80.7 12.2 %collective-permute-start.1 = (bf16[272,128]{1,0:T(8,128)(2,1)S(1)}, bf16[272,128]{1,0:T(8,128)(2,1)S(1)}, u32[]{:S(2)}, u32[]{:S(2)}) collective-permute-start(bf16[272,128]{1,0:T(8,128)(2,1)S(1)} %get-tuple-element.24.own_ref), channel_id=1, source_target_pairs={{0,16},{16,32},{32,48},{48,0},{1,17},{17,33},{33,49},{49,1},{2,18}... | collective-permute-start | bytes 208904 | tf_op jit(solution)/shard_map/ppermute | solution.py:625
  85.0 8.0 %collective-permute-start.2 = (bf16[272,128]{1,0:T(8,128)(2,1)S(1)}, bf16[272,128]{1,0:T(8,128)(2,1)S(1)}, u32[]{:S(2)}, u32[]{:S(2)}) collective-permute-start(bf16[272,128]{1,0:T(8,128)(2,1)S(1)} %get-tuple-element.24.own_ref), channel_id=1, source_target_pairs={{0,32},{16,48},{32,0},{48,16},{1,33},{17,49},{33,1},{49,17},{2,34}... | collective-permute-start | bytes 208904 | tf_op jit(solution)/shard_map/ppermute | solution.py:625
  89.6 6.2 %collective-permute-start.3 = (bf16[272,128]{1,0:T(8,128)(2,1)S(1)}, bf16[272,128]{1,0:T(8,128)(2,1)S(1)}, u32[]{:S(2)}, u32[]{:S(2)}) collective-permute-start(bf16[272,128]{1,0:T(8,128)(2,1)S(1)} %get-tuple-element.24.own_ref), channel_id=1, source_target_pairs={{0,48},{16,0},{32,16},{48,32},{1,49},{17,1},{33,17},{49,33},{2,50}... | collective-permute-start | bytes 208904 | tf_op jit(solution)/shard_map/ppermute | solution.py:625
  95.8 22.9 %copy-start.11 = (s32[160,2]{0,1:T(2,128)S(1)}, s32[160,2]{0,1:T(2,128)}, u32[]{:S(2)}) copy-start(s32[160,2]{0,1:T(2,128)} %param.29) | copy-start | bytes 3844
  95.8 23.1 %copy-start.12 = (f32[160,2]{0,1:T(2,128)S(1)}, f32[160,2]{0,1:T(2,128)}, u32[]{:S(2)}) copy-start(f32[160,2]{0,1:T(2,128)} %param.30) | copy-start | bytes 3844
  96.0 23.0 %copy-start.13 = (f32[256]{0:T(256)S(1)}, f32[256]{0:T(256)}, u32[]{:S(2)}) copy-start(f32[256]{0:T(256)} %param.26) | copy-start | bytes 3076
  96.0 7.1 %collective-permute-start.4 = (bf16[272,128]{1,0:T(8,128)(2,1)S(1)}, bf16[272,128]{1,0:T(8,128)(2,1)S(1)}, u32[]{:S(2)}, u32[]{:S(2)}) collective-permute-start(bf16[272,128]{1,0:T(8,128)(2,1)S(1)} %get-tuple-element.26), channel_id=1, source_target_pairs={{0,64},{64,128},{128,192},{192,256},{256,320},{320,384},{384,448},... | collective-permute-start | bytes 208904 | tf_op jit(solution)/shard_map/ppermute | solution.py:294
  100.2 4.7 %collective-permute-start.5 = (bf16[272,128]{1,0:T(8,128)(2,1)S(1)}, bf16[272,128]{1,0:T(8,128)(2,1)S(1)}, u32[]{:S(2)}, u32[]{:S(2)}) collective-permute-start(bf16[272,128]{1,0:T(8,128)(2,1)S(1)} %get-tuple-element.26), channel_id=1, source_target_pairs={{0,128},{64,192},{128,256},{192,320},{256,384},{320,448},{1,129},{... | collective-permute-start | bytes 208904 | tf_op jit(solution)/shard_map/ppermute | solution.py:294
  105.0 14.2 %collective-permute-start.6 = (bf16[272,128]{1,0:T(8,128)(2,1)S(1)}, bf16[272,128]{1,0:T(8,128)(2,1)S(1)}, u32[]{:S(2)}, u32[]{:S(2)}) collective-permute-start(bf16[272,128]{1,0:T(8,128)(2,1)S(1)} %shard_map.180.after_ref), channel_id=1, source_target_pairs={{0,128},{64,192},{128,256},{192,320},{256,384},{320,448},{1,129},{... | collective-permute-start | bytes 208904 | tf_op jit(solution)/shard_map/ppermute | solution.py:294
  111.2 18.9 %all-to-all-start.2 = ((bf16[32,24,128]{2,1,0:T(8,128)(2,1)}), bf16[32,24,128]{2,1,0:T(8,128)(2,1)S(1)}, u32[]{:S(2)}, u32[]{:S(2)}) async-start(bf16[32,24,128]{2,1,0:T(8,128)(2,1)} %shard_map.190), calls=%async_computation.2 | async-start | bytes 393216 | tf_op jit(solution)/shard_map/all_to_all | solution.py:284
  119.2 9.7 %copy-start.6 = (bf16[256,384]{1,0:T(8,128)(2,1)S(1)}, bf16[256,384]{1,0:T(8,128)(2,1)}, u32[]{:S(2)}) copy-start(bf16[256,384]{1,0:T(8,128)(2,1)} %z_ref.1) | copy-start | bytes 589828
  119.2 9.7 %collective-permute-start.7 = (bf16[272,128]{1,0:T(8,128)(2,1)S(1)}, bf16[272,128]{1,0:T(8,128)(2,1)S(1)}, u32[]{:S(2)}, u32[]{:S(2)}) collective-permute-start(bf16[272,128]{1,0:T(8,128)(2,1)S(1)} %shard_map.181.after_ref), channel_id=1, source_target_pairs={{0,256},{64,320},{128,384},{192,448},{1,257},{65,321},{129,385},{1... | collective-permute-start | bytes 208904 | tf_op jit(solution)/shard_map/ppermute | solution.py:294
